TPU v7x, 512 devices: a whole 4x4x16 slice. The times are simulated.
512 devices in a mesh: sp: 32 (over z, core), tp: 16 (over y, x).
Axes of the slice: x: 4, y: 4, z: 16, core: 2. Of those that a mesh axis runs over, the one named last changes fastest.
Arguments:
- receptance: bfloat16 [8192, 4096], P('sp', 'tp'), may hold values from -6 to 6
- key_vectors: bfloat16 [8192, 4096], P('sp', 'tp'), may hold values from -13 to 13
- value_vectors: bfloat16 [8192, 4096], P('sp', 'tp'), may hold values from -6 to 6
- decay_logits: bfloat16 [8192, 4096], P('sp', 'tp'), may hold values from -20 to 2
- rate_logits: bfloat16 [8192, 4096], P('sp', 'tp'), may hold values from -8 to 4
- gate_logits: bfloat16 [8192, 4096], P('sp', 'tp'), may hold values from -6 to 6
- group_gain: float32 [4096], P('tp'), may hold values from 0.1 to 1.9
- residual: bfloat16 [8192, 4096], P('sp', 'tp'), may hold values from -24 to 24
- mixer_out: bfloat16 [4096, 4096], P(None, 'tp'), may hold values from -0.09375 to 0.09375
- norm_gain: float32 [4096], P('tp'), may hold values from 0.1 to 1.9
- expert_ids: int32 [8192, 2], P('sp'), may hold values from 0 to 31, as said below
- route_weight: float32 [8192, 2], P('sp'), may hold values from 0.25 to 1
- expert_gate: bfloat16 [32, 4096, 1024], P('sp', 'tp'), may hold values from -0.09375 to 0.09375
- expert_up: bfloat16 [32, 4096, 1024], P('sp', 'tp'), may hold values from -0.09375 to 0.09375
- expert_down: bfloat16 [32, 1024, 4096], P('sp', None, 'tp'), may hold values from -0.1875 to 0.1875
Outputs:
- updated: bfloat16 [8192, 4096], P('sp', 'tp')
Inputs may be any that keep to these rules, and one draw needn't show every extreme that they name: `expert_ids`: the experts of a row are different and lie in one group of 8 consecutive experts. In the rows of one index of sp (aligned blocks of 256 rows) no expert is named by more than 32 rows, and in every such block some expert is named by exactly 32 rows.
All inputs are finite; a program needn't handle non-finite values.
Results may differ from a plain program's by a relative error of at most 0.013.
Values may be sent and summed in bfloat16 or wider, within the bound.
A program may use at most 64 MiB of HBM per device.

v0:
```python
import jax
import jax.numpy as jnp
from jax import lax
from jax.experimental import pallas as pl
from jax.experimental.pallas import tpu as pltpu
from jax.sharding import PartitionSpec as P

D = 4096
HEAD = 64
CHUNK = 128
EXP_HALF = 0.6065306597126334


EPS_GROUP = 0.00064
EPS_NORM = 1e-06


def split(x):
    hi = x.astype(jnp.bfloat16)
    lo = (x - hi.astype(jnp.float32)).astype(jnp.bfloat16)
    return hi, lo


def dot(a, b, dims):
    return lax.dot_general(a, b, (dims, ((), ())), preferred_element_type=jnp.float32)


NN = ((1,), (0,))
NT = ((1,), (1,))
TN = ((0,), (0,))


def dot3(a, b, dims=NN):
    return dot(a[0], b[0], dims) + (dot(a[0], b[1], dims) + dot(a[1], b[0], dims))


def dot2(a, b, dims=NN):
    return dot(a[0], b, dims) + dot(a[1], b, dims)


def sigmoid(x):
    return 1.0 / (1.0 + jnp.exp(-x))


def mix_kernel(r_ref, k_ref, v_ref, d_ref, a_ref, out_ref, state_ref):
    tokens = r_ref.shape[0]
    chunks = tokens // CHUNK
    row = lax.broadcasted_iota(jnp.int32, (CHUNK, CHUNK), 0)
    col = lax.broadcasted_iota(jnp.int32, (CHUNK, CHUNK), 1)
    strict = col < row
    causal = col <= row
    eye = jnp.where(col == row, 1.0, 0.0)
    ones_lower = jnp.where(causal, 1.0, 0.0).astype(jnp.bfloat16)
    low = lax.broadcasted_iota(jnp.int32, (CHUNK, 2 * HEAD), 1) < HEAD

    work = []
    for chunk in range(chunks):
        rows = pl.ds(chunk * CHUNK, CHUNK)
        recept = r_ref[rows, :].astype(jnp.float32)
        keyvec = k_ref[rows, :].astype(jnp.float32)
        logdec = -EXP_HALF * sigmoid(d_ref[rows, :].astype(jnp.float32))
        first, second = split(logdec)
        third = (logdec - first.astype(jnp.float32) - second.astype(jnp.float32)).astype(jnp.bfloat16)
        cum_in = dot(ones_lower, first, NN) + (
            dot(ones_lower, second, NN) + dot(ones_lower, third, NN)
        )
        cum_end = cum_in[CHUNK - 1 :, :]
        squares = keyvec * keyvec
        norms = jnp.where(
            low,
            jnp.sum(squares[:, :HEAD], axis=1, keepdims=True),
            jnp.sum(squares[:, HEAD:], axis=1, keepdims=True),
        )
        unit_key = keyvec * lax.rsqrt(1.0 + norms)
        correction = unit_key * sigmoid(a_ref[rows, :].astype(jnp.float32))
        growth = jnp.exp(-cum_in)
        tail = jnp.exp(cum_end - cum_in)
        r_scaled = recept * jnp.exp(cum_in)
        u_scaled = unit_key * jnp.exp(cum_in - logdec)
        queries = split(jnp.concatenate([u_scaled, r_scaled], axis=0))
        sources = split(jnp.concatenate([keyvec * growth, correction * growth], axis=0))
        tails = split(jnp.concatenate([keyvec * tail, -(correction * tail)], axis=0))
        keep = jnp.broadcast_to(jnp.exp(cum_end), (2 * HEAD, 2 * HEAD)).T
        values = v_ref[rows, :]
        for head in range(2):
            lanes = slice(head * HEAD, (head + 1) * HEAD)
            query = tuple(q[:, lanes] for q in queries)
            source = tuple(s[:, lanes] for s in sources)
            scores = dot3(query, source, NT)
            work.append(
                dict(
                    head=head,
                    chunk=chunk,
                    query=query,
                    tail=tuple(t[:, lanes] for t in tails),
                    keep=keep[lanes, :],
                    value=jnp.concatenate(
                        [values[:, lanes], jnp.zeros((CHUNK, HEAD), jnp.bfloat16)], axis=1
                    ),
                    key_both=split(
                        jnp.concatenate(
                            [
                                jnp.where(strict, scores[:CHUNK, :CHUNK], 0.0),
                                jnp.where(causal, scores[CHUNK:, :CHUNK], 0.0),
                            ],
                            axis=0,
                        )
                    ),
                    pull=jnp.where(strict, scores[:CHUNK, CHUNK:], 0.0),
                    corr_read=split(jnp.where(causal, scores[CHUNK:, CHUNK:], 0.0)),
                )
            )
    for item in work:
        item["inverse"] = eye - jnp.where(row // 2 == col // 2, item["pull"], 0.0)
        item["from_values"] = dot2(item["key_both"], item["value"])
    size = 2
    while size < CHUNK:
        joined = (row // (2 * size) == col // (2 * size)) & (row // size != col // size)
        halves = []
        for item in work:
            inverse = split(item["inverse"])
            between = split(jnp.where(joined, item["pull"], 0.0))
            halves.append((inverse, dot3(between, inverse)))
        for item, (inverse, half) in zip(work, halves):
            item["inverse"] = item["inverse"] - dot3(inverse, split(half))
        size *= 2
    key_row = lax.broadcasted_iota(jnp.int32, (HEAD, 2 * HEAD), 0)
    lane = lax.broadcasted_iota(jnp.int32, (HEAD, 2 * HEAD), 1)
    start = jnp.where(lane == key_row + HEAD, 1.0, 0.0)
    states = [start, start]
    for item in work:
        head = item["head"]
        state = states[head]
        from_start = dot3(item["query"], split(state)) + item["from_values"]
        pulled = dot3(split(item["inverse"]), split(from_start[:CHUNK]))
        pulled_parts = split(pulled)
        out_ref[pl.ds(item["chunk"] * CHUNK, CHUNK), pl.ds(head * 2 * HEAD, 2 * HEAD)] = (
            from_start[CHUNK:] - dot3(item["corr_read"], pulled_parts)
        )
        key_tail = tuple(t[:CHUNK] for t in item["tail"])
        corr_tail = tuple(t[CHUNK:] for t in item["tail"])
        states[head] = (
            item["keep"] * state
            + dot2(key_tail, item["value"], TN)
            + dot3(corr_tail, pulled_parts, TN)
        )
    for head in range(2):
        state_ref[pl.ds(head * HEAD, HEAD), :] = states[head].astype(jnp.bfloat16)


def read_kernel(place_ref, read_ref, maps_ref, gate_ref, gain_ref, out_ref):
    def one(step, carried):
        following = []
        for head in range(2):
            both = maps_ref[step, pl.ds(head * HEAD, HEAD), :]
            parts = split(carried[head])
            step_map = both[:, HEAD:]
            following.append(
                both[:, :HEAD].astype(jnp.float32)
                + dot(step_map, parts[0], NN)
                + dot(step_map, parts[1], NN)
            )
        return tuple(following)

    zero = jnp.zeros((HEAD, HEAD), jnp.float32)
    incoming = lax.fori_loop(0, place_ref[0], one, (zero, zero))
    scaled = []
    for head in range(2):
        both = read_ref[:, pl.ds(head * 2 * HEAD, 2 * HEAD)]
        state_read = both[:, :HEAD] + dot3(split(both[:, HEAD:]), split(incoming[head]))
        centred = state_read - jnp.mean(state_read, axis=1, keepdims=True)
        variance = jnp.mean(centred * centred, axis=1, keepdims=True)
        scaled.append(centred * lax.rsqrt(variance + EPS_GROUP))
    gated = (
        jnp.concatenate(scaled, axis=1)
        * gain_ref[...]
        * sigmoid(gate_ref[...].astype(jnp.float32))
    )
    out_ref[...] = gated.astype(jnp.bfloat16)


def time_mix(
    receptance, key_vectors, value_vectors, decay_logits, rate_logits, gate_logits, group_gain
):
    tokens_here, channels = receptance.shape
    pairs = channels // (2 * HEAD)
    wide = pl.BlockSpec((tokens_here, 2 * HEAD), lambda i: (0, i))
    double = pl.BlockSpec((tokens_here, 4 * HEAD), lambda i: (0, i))
    reads, states = pl.pallas_call(
        mix_kernel,
        grid=(pairs,),
        in_specs=[wide] * 5,
        out_specs=[double, pl.BlockSpec((2 * HEAD, 2 * HEAD), lambda i: (i, 0))],
        out_shape=[
            jax.ShapeDtypeStruct((tokens_here, 2 * channels), jnp.float32),
            jax.ShapeDtypeStruct((channels, 2 * HEAD), jnp.bfloat16),
        ],
        name="mix",
    )(receptance, key_vectors, value_vectors, decay_logits, rate_logits)
    maps = lax.all_gather(states, "sp")
    place = lax.axis_index("sp").astype(jnp.int32).reshape(1)
    return pl.pallas_call(
        read_kernel,
        grid=(pairs,),
        in_specs=[
            pl.BlockSpec(memory_space=pltpu.SMEM),
            double,
            pl.BlockSpec((maps.shape[0], 2 * HEAD, 2 * HEAD), lambda i: (0, i, 0)),
            wide,
            pl.BlockSpec((1, 2 * HEAD), lambda i: (0, i)),
        ],
        out_specs=wide,
        out_shape=jax.ShapeDtypeStruct((tokens_here, channels), jnp.bfloat16),
        name="read",
    )(place, reads, maps, gate_logits, group_gain.reshape(1, channels))


def exchange(x, axis, shape, source, target, collective_id, name):
    def kernel(x_ref, out_ref, stage, send_sem, recv_sem, local_sem):
        n = lax.axis_size(axis)
        me = lax.axis_index(axis)
        peers = [lax.rem(me + step, n) for step in range(1, n)]
        barrier = pltpu.get_barrier_semaphore()
        for peer in peers:
            pl.semaphore_signal(
                barrier, inc=1, device_id={axis: peer}, device_id_type=pl.DeviceIdType.MESH
            )
        pl.semaphore_wait(barrier, n - 1)
        copies = []
        for step, peer in enumerate(peers):
            copy = pltpu.make_async_remote_copy(
                src_ref=source(x_ref, peer),
                dst_ref=target(out_ref, me),
                send_sem=send_sem.at[step],
                recv_sem=recv_sem.at[step],
                device_id={axis: peer},
                device_id_type=pl.DeviceIdType.MESH,
            )
            copy.start()
            copies.append(copy)
        own = pltpu.make_async_copy(source(x_ref, me), stage, local_sem)
        own.start()
        own.wait()
        own = pltpu.make_async_copy(stage, target(out_ref, me), local_sem)
        own.start()
        own.wait()
        for copy in copies:
            copy.wait()

    n = lax.axis_size(axis)
    return pl.pallas_call(
        kernel,
        in_specs=[pl.BlockSpec(memory_space=pl.ANY)],
        out_specs=pl.BlockSpec(memory_space=pl.ANY),
        out_shape=jax.ShapeDtypeStruct(shape, x.dtype),
        scratch_shapes=[
            pltpu.VMEM(x.shape[-2:], x.dtype),
            pltpu.SemaphoreType.DMA((n - 1,)),
            pltpu.SemaphoreType.DMA((n - 1,)),
            pltpu.SemaphoreType.DMA,
        ],
        compiler_params=pltpu.CompilerParams(collective_id=collective_id, has_side_effects=True),
        name=name,
    )(x)


def gather_columns(x, axis, collective_id):
    rows, columns = x.shape
    return exchange(
        x,
        axis,
        (rows, lax.axis_size(axis) * columns),
        lambda ref, peer: ref,
        lambda ref, me: ref.at[:, pl.ds(pl.multiple_of(me * columns, columns), columns)],
        collective_id,
        "gather_columns",
    )


def gather_rows(x, axis, collective_id):
    rows, columns = x.shape
    return exchange(
        x,
        axis,
        (lax.axis_size(axis) * rows, columns),
        lambda ref, peer: ref,
        lambda ref, me: ref.at[pl.ds(pl.multiple_of(me * rows, rows), rows), :],
        collective_id,
        "gather_rows",
    )


def swap_blocks(x, axis, collective_id):
    return exchange(
        x, axis, x.shape, lambda ref, peer: ref.at[peer], lambda ref, me: ref.at[me],
        collective_id, "swap_blocks",
    )


def local(
    receptance,
    key_vectors,
    value_vectors,
    decay_logits,
    rate_logits,
    gate_logits,
    group_gain,
    residual,
    mixer_out,
    norm_gain,
    expert_ids,
    route_weight,
    expert_gate,
    expert_up,
    expert_down,
):
    mixed_rows = time_mix(
        receptance, key_vectors, value_vectors, decay_logits, rate_logits, gate_logits, group_gain
    )
    tokens_here, features = residual.shape
    projected = jnp.dot(
        gather_columns(mixed_rows, "tp", 0),
        mixer_out,
        preferred_element_type=jnp.float32,
    )
    midway = (residual.astype(jnp.float32) + projected).astype(jnp.bfloat16)
    midway_f = midway.astype(jnp.float32)
    squares = lax.psum(jnp.sum(midway_f * midway_f, axis=1), "tp")
    inv_rms = lax.rsqrt(squares / D + EPS_NORM)
    normed = (midway_f * norm_gain[None, :] * inv_rms[:, None]).astype(jnp.bfloat16)
    routes = expert_ids.shape[1]
    experts_all = lax.axis_size("sp") * expert_gate.shape[0]
    capacity = 2 * tokens_here * routes // experts_all
    flat_ids = expert_ids.reshape(-1)
    onehot = (flat_ids[:, None] == jnp.arange(experts_all, dtype=jnp.int32)[None, :]).astype(
        jnp.int32
    )
    earlier_count = jnp.sum((jnp.cumsum(onehot, axis=0) - onehot) * onehot, axis=1)
    slot_of = flat_ids * capacity + earlier_count
    owner_token = jnp.arange(tokens_here * routes, dtype=jnp.int32) // routes
    slot_table = (
        jnp.full((experts_all * capacity,), tokens_here, jnp.int32).at[slot_of].set(owner_token)
    )
    padded = jnp.concatenate([normed, jnp.zeros((1, features), jnp.bfloat16)], axis=0)
    outgoing = padded[slot_table].reshape(experts_all, capacity, features)
    arrived = swap_blocks(outgoing, "sp", 2)
    arrived_rows = arrived.reshape(-1, features)
    paired = jnp.concatenate([expert_gate[0], expert_up[0]], axis=1)
    gate_up = lax.psum_scatter(
        jnp.dot(arrived_rows, paired, preferred_element_type=jnp.float32).astype(jnp.bfloat16),
        "tp",
        scatter_dimension=0,
        tiled=True,
    ).astype(jnp.float32)
    half_width = paired.shape[1] // 2
    hidden = (jax.nn.silu(gate_up[:, :half_width]) * gate_up[:, half_width:]).astype(jnp.bfloat16)
    expert_res = jnp.dot(
        gather_rows(hidden, "tp", 1),
        expert_down[0],
        preferred_element_type=jnp.float32,
    )
    returned = swap_blocks(
        expert_res.astype(jnp.bfloat16).reshape(-1, capacity, features), "sp", 3
    )
    picked = (
        returned.reshape(-1, features)[slot_of]
        .astype(jnp.float32)
        .reshape(tokens_here, routes, features)
    )
    routed_sum = jnp.sum(picked * route_weight[:, :, None], axis=1)
    return (midway_f + routed_sum).astype(jnp.bfloat16)


def solution(mesh):
    placed = (
        P("sp", "tp"),
        P("sp", "tp"),
        P("sp", "tp"),
        P("sp", "tp"),
        P("sp", "tp"),
        P("sp", "tp"),
        P("tp"),
        P("sp", "tp"),
        P(None, "tp"),
        P("tp"),
        P("sp", None),
        P("sp", None),
        P("sp", "tp", None),
        P("sp", "tp", None),
        P("sp", None, "tp"),
    )
    return jax.shard_map(
        local, mesh=mesh, in_specs=placed, out_specs=P("sp", "tp"), check_vma=False
    )
```

profile of v0, /device:TPU:1, one launch (start us, length us, event | category | flops | bytes accessed | tf_op | source)
XLA Modules:
  0.0 402.6 jit_solution(910748209022211344)
XLA Ops:
  6.5 0.0 copy-start
  6.5 0.0 all-gather.3.cloned.1.call-start
  6.5 12.0 %mix.1 = (f32[256,512]{1,0:T(8,128)}, bf16[256,128]{1,0:T(8,128)(2,1)}) custom-call(bf16[256,256]{1,0:T(8,128)(2,1)} %r_ref.1, bf16[256,256]{1,0:T(8,128)(2,1)} %k_ref.1, bf16[256,256]{1,0:T(8,128)(2,1)} %v_ref.1, bf16[256,256]{1,0:T(8,128)(2,1)} %d_ref.1, bf16[256,256]{1,0:T(8,128)(2,1)} %a_ref.1), custom_call_target="tpu_custom_call" | custom-call | tf_op jit(solution)/shard_map/mix/pallas_call | solution.py:189
  18.5 0.0 all-gather.3.cloned.1.call-update
  18.6 0.0 reduce-scatter.2.cloned.1.call-start
  18.6 0.8 copy.18
  19.4 0.1 eq.29
  19.6 0.1 eq.25
  19.7 1.2 reduce-window.6
  20.9 0.2 slice_reduce_fusion
  21.2 0.7 broadcast_multiply_fusion
  21.9 0.1 copy.17
  22.0 0.1 mul.60
  22.2 0.1 fusion.9
  22.3 2.4 scatter_custom_fusion
  24.7 71.1 %all-gather.3.cloned.1.call-done = bf16[8192,128]{1,0:T(8,128)(2,1)} async-done(((bf16[256,128]{1,0:T(8,128)(2,1)}), bf16[8192,128]{1,0:T(8,128)(2,1)}) %all-gather.3.cloned.1.call-update) | async-done | bytes 2097168 | tf_op jit(solution)/shard_map/all_gather | solution.py:200
  95.8 0.0 copy-start.6
  95.8 3.6 read.1.x_ref
  99.5 39.0 %gather_columns.1 = bf16[256,4096]{1,0:T(8,128)(2,1)} custom-call(bf16[256,256]{1,0:T(8,128)(2,1)} %read.1.x_ref), custom_call_target="tpu_custom_call" | custom-call | tf_op jit(solution)/shard_map/gather_columns/pallas_call | solution.py:251
  138.4 0.0 copy-done
  138.5 0.0 copy-done.6
  138.5 0.0 copy-start.4
  138.5 2.4 multiply_reduce_fusion.1
  140.9 31.1 %psum.7 = f32[256]{0:T(256)S(1)} all-reduce(f32[256]{0:T(256)S(1)} %get-tuple-element.9), channel_id=1, replica_groups=mesh['sp'=32,'tp'=16] {'tp'}, use_global_device_ids=true, to_apply=%region_1.0 | all-reduce | flops 256 | bytes 2048 | tf_op jit(solution)/shard_map/psum | solution.py:328
  171.9 0.0 copy-done.4
  171.9 0.1 multiply_convert_fusion
  172.1 0.0 copy-start.1
  172.1 0.0 copy-start.2
  172.1 4.9 %gather_fusion = bf16[1024,256]{1,0:T(8,128)(2,1)} fusion(bf16[257,256]{1,0:T(8,128)(2,1)S(1)} %concatenate.6, s32[1024]{0:T(1024)S(1)} %fusion.11), kind=kCustom, calls=%fused_computation | custom fusion | bytes 1052672 | tf_op jit(solution)/shard_map/gather | solution.py:345
  177.0 49.7 %swap_blocks.2 = bf16[32,32,256]{2,1,0:T(8,128)(2,1)} custom-call(bf16[32,32,256]{2,1,0:T(8,128)(2,1)} %bitcast.40), custom_call_target="tpu_custom_call" | custom-call | tf_op jit(solution)/shard_map/swap_blocks/pallas_call | solution.py:251
  226.7 0.0 copy-done.1
  226.7 0.0 copy-done.2
  226.7 4.2 %convolution_convert_fusion = bf16[1024,2048]{1,0:T(8,128)(2,1)} fusion(bf16[1024,256]{1,0:T(8,128)(2,1)} %bitcast.38, bf16[256,1024]{1,0:T(8,128)(2,1)S(1)} %bitcast.42, bf16[256,1024]{1,0:T(8,128)(2,1)S(1)} %bitcast.43), kind=kOutput, calls=%fused_computation.3 | convolution fusion | flops 1077936128 | bytes 5767168 | tf_op jit(solution)/shard_map/dot_general | solution.py:350
  231.0 0.0 copy-start.3
  231.0 0.0 reduce-scatter.2.cloned.1.call-update
  231.0 0.7 copy-done.3
  231.6 0.0 copy-start.5
  231.6 0.1 copy.21
  231.8 85.6 %reduce-scatter.2.cloned.1.call-done = bf16[64,2048]{1,0:T(8,128)(2,1)} async-done(((bf16[1024,2048]{1,0:T(8,128)(2,1)}), bf16[64,2048]{1,0:T(8,128)(2,1)}) %reduce-scatter.2.cloned.1.call-update) | async-done | bytes 262160 | tf_op jit(solution)/shard_map/reduce_scatter | solution.py:349
  317.4 1.0 convert_element_type.48
  318.4 0.7 fusion.6.x_ref
  319.1 30.3 %gather_rows.1 = bf16[1024,1024]{1,0:T(8,128)(2,1)} custom-call(bf16[64,1024]{1,0:T(8,128)(2,1)} %fusion.6.x_ref), custom_call_target="tpu_custom_call" | custom-call | tf_op jit(solution)/shard_map/gather_rows/pallas_call | solution.py:251
  349.4 0.0 copy-done.5
  349.4 3.1 convolution_convert_fusion.1
  352.5 39.0 %swap_blocks.3 = bf16[32,32,256]{2,1,0:T(8,128)(2,1)} custom-call(bf16[32,32,256]{2,1,0:T(8,128)(2,1)} %bitcast.41), custom_call_target="tpu_custom_call" | custom-call | tf_op jit(solution)/shard_map/swap_blocks/pallas_call | solution.py:251
  391.5 2.7 gather_fusion.1
  394.2 0.3 reshape.78
  394.4 0.7 multiply_reduce_fusion
  395.1 0.7 add_convert_fusion
  (9 shorter events, 0.1 us)
Async XLA Ops:
  6.5 131.9 %copy-start = (bf16[4096,256]{1,0:T(8,128)(2,1)S(1)}, bf16[4096,256]{1,0:T(8,128)(2,1)}, u32[]{:S(2)}) copy-start(bf16[4096,256]{1,0:T(8,128)(2,1)} %param.23) | copy-start | bytes 6291460
  6.5 89.3 %all-gather.3.cloned.1.call-start = ((), (), s32[]{:S(2)}) async-start(), calls=%async_computation.2 | async-start | bytes 2162688 | tf_op jit(solution)/shard_map/all_gather | solution.py:200
  18.6 298.8 %reduce-scatter.2.cloned.1.call-start = ((), (), s32[]{:S(2)}) async-start(), calls=%async_computation.1 | async-start | bytes 4456448 | tf_op jit(solution)/shard_map/reduce_scatter | solution.py:349
  95.8 42.6 %copy-start.6 = (bf16[256,256]{1,0:T(8,128)(2,1)S(1)}, bf16[256,256]{1,0:T(8,128)(2,1)}, u32[]{:S(2)}) copy-start(bf16[256,256]{1,0:T(8,128)(2,1)} %param.22) | copy-start | bytes 393220
  138.5 33.5 %copy-start.4 = (f32[256]{0:T(256)S(1)}, f32[256]{0:T(256)}, u32[]{:S(2)}) copy-start(f32[256]{0:T(256)} %param.24) | copy-start | bytes 3076
  172.1 54.7 %copy-start.1 = (bf16[1,256,1024]{2,1,0:T(8,128)(2,1)S(1)}, bf16[1,256,1024]{2,1,0:T(8,128)(2,1)}, u32[]{:S(2)}) copy-start(bf16[1,256,1024]{2,1,0:T(8,128)(2,1)} %param.28) | copy-start | bytes 1572868
  172.1 54.7 %copy-start.2 = (bf16[1,256,1024]{2,1,0:T(8,128)(2,1)S(1)}, bf16[1,256,1024]{2,1,0:T(8,128)(2,1)}, u32[]{:S(2)}) copy-start(bf16[1,256,1024]{2,1,0:T(8,128)(2,1)} %param.27) | copy-start | bytes 1572868
  231.0 0.7 copy-start.3
  231.6 117.8 %copy-start.5 = (bf16[1,1024,256]{2,1,0:T(8,128)(2,1)S(1)}, bf16[1,1024,256]{2,1,0:T(8,128)(2,1)}, u32[]{:S(2)}) copy-start(bf16[1,1024,256]{2,1,0:T(8,128)(2,1)} %param.29) | copy-start | bytes 1572868
Sparse Core Ops, SparseCore 0:
  18.7 77.1 all-gather.2
  231.1 86.2 reduce-scatter.1
where the time goes:
time: 403 us
  Pallas kernels  174 us (43%)
  waiting for transfers between devices  157 us (39%)
  blocking collectives  31.1 us (8%)
  between operations  13.6 us (3%)
  local copies, waits for them, and re-layouts  12.8 us (3%)
  matrix products  9.71 us (2%)
  other arithmetic  5.25 us (1%)
    pallas_call x4, Pallas kernels, exchange(): pl.pallas_call(kernel, in_specs=[pl.BlockSpec(memory_space=pl.ANY)], out_...  158 us
    reduce_scatter x1, waiting for transfers between devices, local(): lax.psum_scatter(jnp.dot(arrived_rows, paired, preferred_element_type=jnp...  85.6 us
    all_gather x1, waiting for transfers between devices, time_mix(): maps = lax.all_gather(states, 'sp')  71.1 us
    psum x1, blocking collectives, local(): squares = lax.psum(jnp.sum(midway_f * midway_f, axis=1), 'tp')  31.1 us
    pallas_call x1, Pallas kernels, time_mix(): pl.pallas_call(mix_kernel, grid=(pairs,), in_specs=[wide] * 5, out_specs=...  12 us
  transfers between devices with their start and end apart: 2, of which 2 were waited for; matrix products, arithmetic and copies ran while one was open for 2% of the time, Pallas kernels for 0%

commit v1 on v0

v1 whole, which is shorter than its diff:
```python
import functools

import jax
import jax.numpy as jnp
from jax import lax
from jax.experimental import pallas as pl
from jax.experimental.pallas import tpu as pltpu
from jax.sharding import PartitionSpec as P

D = 4096
HEAD = 64
CHUNK = 128
EXP_HALF = 0.6065306597126334

NZ = 16
N_SP = 2 * NZ
SIDE = 4
N_TP = SIDE * SIDE
CAP = 32
PARTS = 4
POS = N_SP // PARTS
SUB = POS * CAP // N_TP

EPS_GROUP = 0.00064
EPS_NORM = 1e-06
MESH = pl.DeviceIdType.MESH

OFFSETS = [0]
for _near in range(1, NZ // 2):
    OFFSETS += [_near, -_near]
OFFSETS += [NZ // 2]
INVERSE = [OFFSETS.index(-o if o != NZ // 2 else o) for o in OFFSETS]


def split(x):
    hi = x.astype(jnp.bfloat16)
    lo = (x - hi.astype(jnp.float32)).astype(jnp.bfloat16)
    return hi, lo


def dot(a, b, dims):
    return lax.dot_general(a, b, (dims, ((), ())), preferred_element_type=jnp.float32)


NN = ((1,), (0,))
NT = ((1,), (1,))
TN = ((0,), (0,))


def dot3(a, b, dims=NN):
    return dot(a[0], b[0], dims) + (dot(a[0], b[1], dims) + dot(a[1], b[0], dims))


def dot2(a, b, dims=NN):
    return dot(a[0], b, dims) + dot(a[1], b, dims)


def sigmoid(x):
    return 1.0 / (1.0 + jnp.exp(-x))


def mix_kernel(r_ref, k_ref, v_ref, d_ref, a_ref, out_ref, state_ref):
    tokens = r_ref.shape[0]
    chunks = tokens // CHUNK
    row = lax.broadcasted_iota(jnp.int32, (CHUNK, CHUNK), 0)
    col = lax.broadcasted_iota(jnp.int32, (CHUNK, CHUNK), 1)
    strict = col < row
    causal = col <= row
    eye = jnp.where(col == row, 1.0, 0.0)
    ones_lower = jnp.where(causal, 1.0, 0.0).astype(jnp.bfloat16)
    low = lax.broadcasted_iota(jnp.int32, (CHUNK, 2 * HEAD), 1) < HEAD

    work = []
    for chunk in range(chunks):
        rows = pl.ds(chunk * CHUNK, CHUNK)
        recept = r_ref[rows, :].astype(jnp.float32)
        keyvec = k_ref[rows, :].astype(jnp.float32)
        logdec = -EXP_HALF * sigmoid(d_ref[rows, :].astype(jnp.float32))
        first, second = split(logdec)
        third = (logdec - first.astype(jnp.float32) - second.astype(jnp.float32)).astype(jnp.bfloat16)
        cum_in = dot(ones_lower, first, NN) + (
            dot(ones_lower, second, NN) + dot(ones_lower, third, NN)
        )
        cum_end = cum_in[CHUNK - 1 :, :]
        squares = keyvec * keyvec
        norms = jnp.where(
            low,
            jnp.sum(squares[:, :HEAD], axis=1, keepdims=True),
            jnp.sum(squares[:, HEAD:], axis=1, keepdims=True),
        )
        unit_key = keyvec * lax.rsqrt(1.0 + norms)
        correction = unit_key * sigmoid(a_ref[rows, :].astype(jnp.float32))
        growth = jnp.exp(-cum_in)
        tail = jnp.exp(cum_end - cum_in)
        r_scaled = recept * jnp.exp(cum_in)
        u_scaled = unit_key * jnp.exp(cum_in - logdec)
        queries = split(jnp.concatenate([u_scaled, r_scaled], axis=0))
        sources = split(jnp.concatenate([keyvec * growth, correction * growth], axis=0))
        tails = split(jnp.concatenate([keyvec * tail, -(correction * tail)], axis=0))
        keep = jnp.broadcast_to(jnp.exp(cum_end), (2 * HEAD, 2 * HEAD)).T
        values = v_ref[rows, :]
        for head in range(2):
            lanes = slice(head * HEAD, (head + 1) * HEAD)
            query = tuple(q[:, lanes] for q in queries)
            source = tuple(s[:, lanes] for s in sources)
            scores = dot3(query, source, NT)
            work.append(
                dict(
                    head=head,
                    chunk=chunk,
                    query=query,
                    tail=tuple(t[:, lanes] for t in tails),
                    keep=keep[lanes, :],
                    value=jnp.concatenate(
                        [values[:, lanes], jnp.zeros((CHUNK, HEAD), jnp.bfloat16)], axis=1
                    ),
                    key_both=split(
                        jnp.concatenate(
                            [
                                jnp.where(strict, scores[:CHUNK, :CHUNK], 0.0),
                                jnp.where(causal, scores[CHUNK:, :CHUNK], 0.0),
                            ],
                            axis=0,
                        )
                    ),
                    pull=jnp.where(strict, scores[:CHUNK, CHUNK:], 0.0),
                    corr_read=split(jnp.where(causal, scores[CHUNK:, CHUNK:], 0.0)),
                )
            )
    for item in work:
        item["inverse"] = eye - jnp.where(row // 2 == col // 2, item["pull"], 0.0)
        item["from_values"] = dot2(item["key_both"], item["value"])
    size = 2
    while size < CHUNK:
        joined = (row // (2 * size) == col // (2 * size)) & (row // size != col // size)
        halves = []
        for item in work:
            inverse = split(item["inverse"])
            between = split(jnp.where(joined, item["pull"], 0.0))
            halves.append((inverse, dot3(between, inverse)))
        for item, (inverse, half) in zip(work, halves):
            item["inverse"] = item["inverse"] - dot3(inverse, split(half))
        size *= 2
    key_row = lax.broadcasted_iota(jnp.int32, (HEAD, 2 * HEAD), 0)
    lane = lax.broadcasted_iota(jnp.int32, (HEAD, 2 * HEAD), 1)
    start = jnp.where(lane == key_row + HEAD, 1.0, 0.0)
    states = [start, start]
    for item in work:
        head = item["head"]
        state = states[head]
        from_start = dot3(item["query"], split(state)) + item["from_values"]
        pulled = dot3(split(item["inverse"]), split(from_start[:CHUNK]))
        pulled_parts = split(pulled)
        out_ref[pl.ds(item["chunk"] * CHUNK, CHUNK), pl.ds(head * 2 * HEAD, 2 * HEAD)] = (
            from_start[CHUNK:] - dot3(item["corr_read"], pulled_parts)
        )
        key_tail = tuple(t[:CHUNK] for t in item["tail"])
        corr_tail = tuple(t[CHUNK:] for t in item["tail"])
        states[head] = (
            item["keep"] * state
            + dot2(key_tail, item["value"], TN)
            + dot3(corr_tail, pulled_parts, TN)
        )
    for head in range(2):
        state_ref[pl.ds(head * HEAD, HEAD), :] = states[head].astype(jnp.bfloat16)


def mix(receptance, key_vectors, value_vectors, decay_logits, rate_logits):
    tokens_here, channels = receptance.shape
    pairs = channels // (2 * HEAD)
    wide = pl.BlockSpec((tokens_here, 2 * HEAD), lambda i: (0, i))
    double = pl.BlockSpec((tokens_here, 4 * HEAD), lambda i: (0, i))
    return pl.pallas_call(
        mix_kernel,
        grid=(pairs,),
        in_specs=[wide] * 5,
        out_specs=[double, pl.BlockSpec((2 * HEAD, 2 * HEAD), lambda i: (i, 0))],
        out_shape=[
            jax.ShapeDtypeStruct((tokens_here, 2 * channels), jnp.float32),
            jax.ShapeDtypeStruct((channels, 2 * HEAD), jnp.bfloat16),
        ],
        name="mix",
    )(receptance, key_vectors, value_vectors, decay_logits, rate_logits)


def route_kernel(place_ref, ids_ref, weight_ref, pick_ref, high_ref, low_ref):
    tokens = ids_ref.shape[0]
    slots = N_SP * CAP
    expert = lax.broadcasted_iota(jnp.int32, (tokens, 128), 1)
    named = [ids_ref[:, k : k + 1] == expert for k in range(2)]
    onehot = jnp.where(named[0] | named[1], 1.0, 0.0).astype(jnp.bfloat16)
    row = lax.broadcasted_iota(jnp.int32, (tokens, tokens), 0)
    col = lax.broadcasted_iota(jnp.int32, (tokens, tokens), 1)
    before = jnp.where(col < row, 1.0, 0.0).astype(jnp.bfloat16)
    earlier = dot(before, onehot, NN).astype(jnp.bfloat16)
    weight = jnp.where(named[0], weight_ref[:, 0:1], 0.0) + jnp.where(named[1], weight_ref[:, 1:2], 0.0)
    high, low = split(weight)
    slot = lax.broadcasted_iota(jnp.int32, (128, slots), 1)
    source = lax.broadcasted_iota(jnp.int32, (128, slots), 0)
    near = slot // (2 * CAP)
    step = (near + 1) // 2
    off = jnp.where(near % 2 == 1, step, NZ - step)
    chip = (place_ref[0] // 2 + off) % NZ
    core = (place_ref[0] + slot // CAP) % 2
    spread = jnp.where(source == chip * 2 + core, 1.0, 0.0).astype(jnp.bfloat16)
    rank = (lax.broadcasted_iota(jnp.int32, (tokens, slots), 1) % CAP).astype(jnp.float32)
    taken = jnp.where(dot(earlier, spread, NN) == rank, dot(onehot, spread, NN), 0.0)
    pick_ref[...] = taken.T.astype(jnp.bfloat16)
    high_ref[...] = (taken * dot(high, spread, NN)).astype(jnp.bfloat16)
    low_ref[...] = (taken * dot(low, spread, NN)).astype(jnp.bfloat16)


def route(expert_ids, route_weight):
    tokens = expert_ids.shape[0]
    slots = N_SP * CAP
    place = lax.axis_index("sp").astype(jnp.int32).reshape(1)
    return pl.pallas_call(
        route_kernel,
        in_specs=[
            pl.BlockSpec(memory_space=pltpu.SMEM),
            pl.BlockSpec(memory_space=pltpu.VMEM),
            pl.BlockSpec(memory_space=pltpu.VMEM),
        ],
        out_shape=[
            jax.ShapeDtypeStruct((slots, tokens), jnp.bfloat16),
            jax.ShapeDtypeStruct((tokens, slots), jnp.bfloat16),
            jax.ShapeDtypeStruct((tokens, slots), jnp.bfloat16),
        ],
        name="route",
    )(place, expert_ids, route_weight)


class Place:
    def __init__(self):
        self.sp = lax.axis_index("sp")
        self.tp = lax.axis_index("tp")
        self.z, self.core = self.sp // 2, self.sp % 2
        self.y, self.x = self.tp // SIDE, self.tp % SIDE

    def chip(self, off, other=False):
        core = (self.core + 1) % 2 if other else self.core
        return ((self.z + off + NZ) % NZ) * 2 + core

    def at_z(self, off, other=False):
        return {"sp": self.chip(off, other), "tp": self.tp}

    def along(self, axis, off):
        if axis == "x":
            return {"sp": self.sp, "tp": self.y * SIDE + (self.x + off + SIDE) % SIDE}
        return {"sp": self.sp, "tp": ((self.y + off + SIDE) % SIDE) * SIDE + self.x}

    def on(self, axis, off=0):
        return ((self.x if axis == "x" else self.y) + off + SIDE) % SIDE


class Copies:
    def __init__(self, send, recv):
        self.send, self.recv = send, recv
        self.made = []

    def __call__(self, src, dst, device):
        index = len(self.made)
        copy = pltpu.make_async_remote_copy(
            src_ref=src,
            dst_ref=dst,
            send_sem=self.send.at[index],
            recv_sem=self.recv.at[index],
            device_id=device,
            device_id_type=MESH,
        )
        self.made.append(copy)
        return copy

    def drain(self):
        for copy in self.made:
            copy.wait_send()


def greet(devices):
    barrier = pltpu.get_barrier_semaphore()
    for device in devices:
        pl.semaphore_signal(barrier, inc=1, device_id=device, device_id_type=MESH)
    return lambda: pl.semaphore_wait(barrier, len(devices))


ORDER = (("x", "y"), ("y", "x"))


class TorusGather:
    def __init__(self, place, copies, blocks):
        self.place, self.copies, self.blocks = place, copies, blocks
        self.state = [dict() for _ in blocks]

    def own(self, h):
        first, second = ORDER[h]
        return self.place.on(second) * SIDE + self.place.on(first)

    def exchange(self, h, axis, mine):
        up, down = self.place.along(axis, 1), self.place.along(axis, -1)
        whole = mine(0)
        direct = [self.copies(whole, whole, up), self.copies(whole, whole, down)]
        for copy in direct:
            copy.start()
        return direct, up, down

    def relay(self, direct, up, down, mine, half):
        passed = []
        for side, (copy, off, target) in enumerate(zip(direct, (-1, 1), (up, down))):
            copy.wait_recv()
            piece = half(mine(off), side)
            passed.append(self.copies(piece, piece, target))
            passed[-1].start()
        return passed

    def stage(self, n, h):
        first, second = ORDER[h]
        place, block, s = self.place, self.blocks[h], self.state[h]

        def one(off):
            return block.at[place.on(second) * SIDE + place.on(first, off)]

        def four(off):
            return block.at[pl.ds(place.on(second, off) * SIDE, SIDE)]

        if n == 0:
            s["a"] = self.exchange(h, first, one)
        elif n == 1:
            s["b"] = self.relay(*s["a"], one, lambda ref, side: ref.at[side])
        elif n == 2:
            for copy in s["b"]:
                copy.wait_recv()
            s["c"] = self.exchange(h, second, four)
        elif n == 3:
            s["d"] = self.relay(*s["c"], four, lambda ref, side: ref.at[:, side])
        else:
            for copy in s["d"]:
                copy.wait_recv()


def torus_order(h):
    if h == 0:
        return list(range(N_TP))
    return [x * SIDE + y for y in range(SIDE) for x in range(SIDE)]


def front_kernel(
    reads_ref, states_ref, gate_ref, gain_ref, weight_ref, residual_ref,
    out_ref, maps, half_a, half_b, send, recv,
):
    place = Place()
    copies = Copies(send, recv)
    partner = place.at_z(0, True)
    up, down = place.at_z(1), place.at_z(-1)
    neighbours = [partner, up, down] + [place.along(axis, off) for axis in "xy" for off in (1, -1)]
    wait = greet(neighbours)
    tokens = out_ref.shape[0]
    pieces = 2
    rows = states_ref.shape[0] // pieces
    maps[place.sp] = states_ref[...]
    wait()

    def slot(off):
        return place.chip(off)

    def hop(n, direction, piece):
        part = pl.ds(piece * rows, rows)
        target = up if direction > 0 else down
        here = slot(-direction * (n - 1))
        src = states_ref.at[part] if n == 1 else maps.at[here, part]
        copy = copies(src, maps.at[here, part], target)
        copy.start()
        return copy

    across = [copies(states_ref, maps.at[slot(0)], partner)]
    last = {1: NZ // 2, -1: NZ // 2 - 1}
    current = {}
    for piece in range(pieces):
        for direction in (1, -1):
            current[direction, piece] = hop(1, direction, piece)
    across[0].start()
    for n in range(1, NZ // 2 + 1):
        for piece in range(pieces):
            for direction in (1, -1):
                if n > last[direction]:
                    continue
                current[direction, piece].wait_recv()
                if n < last[direction]:
                    current[direction, piece] = hop(n + 1, direction, piece)
        for direction in (1, -1):
            if n <= last[direction]:
                here = slot(-direction * n)
                copy = copies(maps.at[here], maps.at[here], partner)
                copy.start()
                across.append(copy)
    for copy in across:
        copy.wait_recv()

    heads = states_ref.shape[0] // HEAD

    def fold(step, carried):
        following = []
        for head in range(heads):
            both = maps[step, pl.ds(head * HEAD, HEAD), :]
            hi, lo = split(carried[head])
            step_map = both[:, HEAD:]
            following.append(
                both[:, :HEAD].astype(jnp.float32) + dot(step_map, hi, NN) + dot(step_map, lo, NN)
            )
        return tuple(following)

    zero = jnp.zeros((HEAD, HEAD), jnp.float32)
    incoming = lax.fori_loop(0, place.sp, fold, (zero,) * heads)
    scaled = []
    for head in range(heads):
        both = reads_ref[:, pl.ds(head * 2 * HEAD, 2 * HEAD)]
        state_read = both[:, :HEAD] + dot3(split(both[:, HEAD:]), split(incoming[head]))
        centred = state_read - jnp.mean(state_read, axis=1, keepdims=True)
        variance = jnp.mean(centred * centred, axis=1, keepdims=True)
        scaled.append(centred * lax.rsqrt(variance + EPS_GROUP))
    gated = (
        jnp.concatenate(scaled, axis=1)
        * gain_ref[...]
        * sigmoid(gate_ref[...].astype(jnp.float32))
    ).astype(jnp.bfloat16)
    halves = (half_a, half_b)
    gather = TorusGather(place, copies, halves)
    quarter = tokens // 4
    for h in range(2):
        for q in range(2):
            at = (2 * h + q) * quarter
            halves[h][gather.own(h), q] = gated[at : at + quarter]
    for n in range(5):
        for h in range(2):
            gather.stage(n, h)
    width = gated.shape[1]
    for h in range(2):
        total = jnp.zeros((tokens // 2, out_ref.shape[1]), jnp.float32)
        for t, at in enumerate(torus_order(h)):
            block = halves[h][at].reshape(tokens // 2, width)
            total += dot(block, weight_ref[pl.ds(t * width, width), :], NN)
        part = pl.ds(h * (tokens // 2), tokens // 2)
        out_ref[part, :] = (residual_ref[part, :].astype(jnp.float32) + total).astype(jnp.bfloat16)
    copies.drain()


def front(reads, states, gate_logits, group_gain, mixer_out, residual):
    tokens, channels = gate_logits.shape
    quarter = tokens // 4
    count = 64
    vmem = pl.BlockSpec(memory_space=pltpu.VMEM)
    return pl.pallas_call(
        front_kernel,
        in_specs=[vmem] * 6,
        out_specs=vmem,
        out_shape=jax.ShapeDtypeStruct(residual.shape, jnp.bfloat16),
        scratch_shapes=[
            pltpu.VMEM((N_SP, *states.shape), jnp.bfloat16),
            pltpu.VMEM((N_TP, 2, quarter, channels), jnp.bfloat16),
            pltpu.VMEM((N_TP, 2, quarter, channels), jnp.bfloat16),
            pltpu.SemaphoreType.DMA((count,)),
            pltpu.SemaphoreType.DMA((count,)),
        ],
        compiler_params=pltpu.CompilerParams(collective_id=0, has_side_effects=True),
        name="front",
    )(reads, states, gate_logits, group_gain.reshape(1, channels), mixer_out, residual)


EXTRA = 128


def widths(ff):
    return ((ff // 2 + EXTRA, ff // 2), (ff // 2, ff // 2))


def back_scratch(ff, features):
    wide = widths(ff)
    per_part = []
    for h in range(2):
        for q in range(2):
            w = wide[h][q]
            per_part += [
                pltpu.VMEM((PARTS, N_TP, SUB, w), jnp.bfloat16),
                pltpu.VMEM((PARTS, SIDE, SUB, w), jnp.bfloat16),
                pltpu.VMEM((PARTS, 2, SIDE, SUB, w), jnp.bfloat16),
                pltpu.VMEM((PARTS, SIDE, SUB, w), jnp.bfloat16),
                pltpu.VMEM((PARTS, SUB, w), jnp.bfloat16),
                pltpu.VMEM((PARTS, 2, SUB, w), jnp.bfloat16),
            ]
    hidden = [pltpu.VMEM((PARTS, N_TP, 2, SUB, ff // 4), jnp.bfloat16) for _ in range(2)]
    slots = [pltpu.VMEM((N_SP, CAP, features), jnp.bfloat16) for _ in range(4)]
    count = 2 * (N_SP - 1) + PARTS * (24 + 16)
    return slots + hidden + per_part + [
        pltpu.SemaphoreType.DMA((count,)),
        pltpu.SemaphoreType.DMA((count,)),
    ]


REDUCE = (("y", "x"), ("x", "y"))


def back_kernel(
    mid_ref, gain_ref, pick_ref, high_ref, low_ref, gate_ref, up_ref, down_ref, out_ref, *scratch
):
    outgoing, arrived, results, returned = scratch[:4]
    hidden = scratch[4:6]
    buffers = [[scratch[6 + (2 * h + q) * 6 : 12 + (2 * h + q) * 6] for q in range(2)] for h in range(2)]
    send, recv = scratch[30:]
    place = Place()
    copies = Copies(send, recv)
    features = mid_ref.shape[1]
    ff = gate_ref.shape[1]
    half = ff // 2
    z_peers = [
        (2 * near + other, 2 * INVERSE[near] + other, place.at_z(off, bool(other)))
        for near, off in enumerate(OFFSETS)
        for other in range(2)
        if off != 0 or other
    ]
    ring = [place.along(axis, off) for axis in "xy" for off in (1, -1)]
    wait = greet([peer[2] for peer in z_peers] + ring)
    for part in range(PARTS):
        rows = pl.ds(part * POS * CAP, POS * CAP)
        outgoing[pl.ds(part * POS, POS)] = (
            dot(pick_ref[rows, :], mid_ref[...], NN).astype(jnp.bfloat16).reshape(POS, CAP, features)
        )
    arrived[0] = outgoing[0]
    wait()
    dispatch = {}
    for at, there, device in z_peers:
        dispatch[at] = copies(outgoing.at[at], arrived.at[there], device)
        dispatch[at].start()
    lands = {there: dispatch[at] for at, there, _ in z_peers}
    back = {}
    state = [dict() for _ in range(PARTS)]
    gathers = [
        TorusGather(place, copies, [hidden[h].at[part] for h in range(2)]) for part in range(PARTS)
    ]

    def add(*refs):
        total = refs[0].astype(jnp.float32)
        for ref in refs[1:]:
            total += ref.astype(jnp.float32)
        return total

    def relay_out(part, h, level):
        axis = REDUCE[h][level]
        far = place.on(axis, 2)
        sent = []
        for q, off in ((0, 1), (1, -1)):
            product, passed1, _, reduced, passed2, _ = buffers[h][q]
            if level == 0:
                src, dst = product.at[part, pl.ds(far * SIDE, SIDE)], passed1.at[part]
            else:
                src, dst = reduced.at[part, far], passed2.at[part]
            copy = copies(src, dst, place.along(axis, off))
            copy.start()
            sent.append(copy)
        state[part][h, level, "relay"] = sent

    def join(part, h, level):
        axis = REDUCE[h][level]
        sent = []
        for side, off in ((0, 1), (1, -1)):
            state[part][h, level, "relay"][side].wait_recv()
            near = place.on(axis, off)
            for q in (side, 1 - side):
                product, passed1, both1, reduced, passed2, both2 = buffers[h][q]
                if level == 0:
                    at, mine, dst = pl.ds(near * SIDE, SIDE), product, both1.at[part, side]
                    other = passed1
                else:
                    at, mine, dst = near, reduced, both2.at[part, side]
                    other = passed2
                if q == side:
                    mine[part, at] = add(mine[part, at], other[part]).astype(jnp.bfloat16)
                copy = copies(mine.at[part, at], dst, place.along(axis, off))
                copy.start()
                sent.append(copy)
        state[part][h, level, "both"] = sent

    def finish(part, h, level):
        axis = REDUCE[h][level]
        for copy in state[part][h, level, "both"]:
            copy.wait_recv()
        here = place.on(axis)
        totals = []
        for q in range(2):
            product, _, both1, reduced, _, both2 = buffers[h][q]
            if level == 0:
                total = add(product[part, pl.ds(here * SIDE, SIDE)], both1[part, 0], both1[part, 1])
                reduced[part] = total.astype(jnp.bfloat16)
            else:
                totals.append(add(reduced[part, here], both2[part, 0], both2[part, 1]))
        return totals

    def products(part):
        for at in range(part * POS, (part + 1) * POS):
            if at in lands:
                lands[at].wait_recv()
        rows = arrived[pl.ds(part * POS, POS)].reshape(POS * CAP, features).astype(jnp.float32)
        squares = jnp.sum(rows * rows, axis=1, keepdims=True)
        extra = jnp.broadcast_to(squares, (POS * CAP, EXTRA)).astype(jnp.bfloat16)
        scaled = (rows * gain_ref[...]).astype(jnp.bfloat16)
        for h in range(2):
            for q, matrix in enumerate((gate_ref, up_ref)):
                value = dot(scaled, matrix[:, pl.ds(h * half, half)], NN).astype(jnp.bfloat16)
                value = value.reshape(N_TP, SUB, half)
                product = buffers[h][q][0]
                for t, at in enumerate(torus_order(h)):
                    product[part, at, :, pl.ds(0, half)] = value[t]
                    if h == 0 and q == 0:
                        product[part, at, :, pl.ds(half, EXTRA)] = extra[t * SUB : (t + 1) * SUB]
            relay_out(part, h, 0)

    def activate(part):
        (gate_a, up_a), (gate_b, up_b) = [finish(part, h, 1) for h in range(2)]
        inv = lax.rsqrt(gate_a[:, half : half + 1] * (1.0 / D) + EPS_NORM)
        gather = gathers[part]
        for h, (gate, up) in enumerate(((gate_a[:, :half], up_a), (gate_b, up_b))):
            gate = gate * inv
            value = (gate * sigmoid(gate) * (up * inv)).astype(jnp.bfloat16)
            for q in range(2):
                hidden[h][part, gather.own(h), q] = value[:, q * (half // 2) : (q + 1) * (half // 2)]
            gather.stage(0, h)

    def outputs(part):
        total = jnp.zeros((POS * CAP, features), jnp.float32)
        for h in range(2):
            gathers[part].stage(4, h)
            for q in range(2):
                blocks = [hidden[h][part, at, q] for at in torus_order(h)]
                at = h * half + q * (half // 2)
                total += dot(jnp.concatenate(blocks, axis=0), down_ref[pl.ds(at, half // 2), :], NN)
        results[pl.ds(part * POS, POS)] = total.astype(jnp.bfloat16).reshape(POS, CAP, features)
        for at, there, device in z_peers:
            if part * POS <= at < (part + 1) * POS:
                back[at] = copies(results.at[at], returned.at[there], device)
                back[at].start()
        if part == 0:
            returned[0] = results[0]

    def both(action):
        def run(part):
            for h in range(2):
                action(part, h)
        return run

    stages = [
        products,
        both(lambda part, h: join(part, h, 0)),
        both(lambda part, h: (finish(part, h, 0), relay_out(part, h, 1))),
        both(lambda part, h: join(part, h, 1)),
        activate,
        both(lambda part, h: gathers[part].stage(1, h)),
        both(lambda part, h: gathers[part].stage(2, h)),
        both(lambda part, h: gathers[part].stage(3, h)),
        outputs,
    ]
    begins = (0.0, 5.0, 12.0, 21.0)
    plan = sorted(
        (begins[part] + 3.0 * n, part, n) for part in range(PARTS) for n in range(len(stages))
    )
    for _, part, n in plan:
        stages[n](part)

    came = {there: back[at] for at, there, _ in z_peers}
    total = mid_ref[...].astype(jnp.float32)
    for part in range(PARTS):
        for at in range(part * POS, (part + 1) * POS):
            if at in came:
                came[at].wait_recv()
        rows = returned[pl.ds(part * POS, POS)].reshape(POS * CAP, features)
        columns = pl.ds(part * POS * CAP, POS * CAP)
        total += dot(high_ref[:, columns], rows, NN) + dot(low_ref[:, columns], rows, NN)
    out_ref[...] = total.astype(jnp.bfloat16)
    copies.drain()


def back(midway, norm_gain, pick, high, low, gate, up, down):
    features = midway.shape[1]
    vmem = pl.BlockSpec(memory_space=pltpu.VMEM)
    return pl.pallas_call(
        back_kernel,
        in_specs=[vmem] * 8,
        out_specs=vmem,
        out_shape=jax.ShapeDtypeStruct(midway.shape, jnp.bfloat16),
        scratch_shapes=back_scratch(gate.shape[1], features),
        compiler_params=pltpu.CompilerParams(collective_id=1, has_side_effects=True),
        name="back",
    )(midway, norm_gain.reshape(1, features), pick, high, low, gate, up, down)


def local(
    receptance,
    key_vectors,
    value_vectors,
    decay_logits,
    rate_logits,
    gate_logits,
    group_gain,
    residual,
    mixer_out,
    norm_gain,
    expert_ids,
    route_weight,
    expert_gate,
    expert_up,
    expert_down,
):
    reads, states = mix(receptance, key_vectors, value_vectors, decay_logits, rate_logits)
    pick, high, low = route(expert_ids, route_weight)
    midway = front(reads, states, gate_logits, group_gain, mixer_out, residual)
    return back(midway, norm_gain, pick, high, low, expert_gate[0], expert_up[0], expert_down[0])


def solution(mesh):
    placed = (
        P("sp", "tp"),
        P("sp", "tp"),
        P("sp", "tp"),
        P("sp", "tp"),
        P("sp", "tp"),
        P("sp", "tp"),
        P("tp"),
        P("sp", "tp"),
        P(None, "tp"),
        P("tp"),
        P("sp", None),
        P("sp", None),
        P("sp", "tp", None),
        P("sp", "tp", None),
        P("sp", None, "tp"),
    )
    return jax.shard_map(
        local, mesh=mesh, in_specs=placed, out_specs=P("sp", "tp"), check_vma=False
    )
```

time: 403 us -> 186 us (0.46)
  waiting for transfers between devices: 157 us -> 0 us
  blocking collectives: 31.1 us -> 0 us
  between operations: 13.6 us -> 0.02 us
  matrix products: 9.71 us -> 0 us
  local copies, waits for them, and re-layouts: 12.8 us -> 4.51 us
  Pallas kernels: 174 us -> 181 us
  other arithmetic: 5.25 us -> 0 us
    reduce_scatter x1 -> x0, waiting for transfers between devices: 85.6 us -> none  [local(): lax.psum_scatter(jnp.dot(arrived_rows, paired, preferred_element_type=jnp...]
    all_gather x1 -> x0, waiting for transfers between devices: 71.1 us -> none  [time_mix(): maps = lax.all_gather(states, 'sp')]
    psum x1 -> x0, blocking collectives: 31.1 us -> none  [local(): squares = lax.psum(jnp.sum(midway_f * midway_f, axis=1), 'tp')]
    dot_general x3 -> x0, matrix products: 9.71 us -> none  [the longest x1 4.23 us: local(): jnp.dot(arrived_rows, paired, preferred_element_type=jnp.float32)]
    pallas_call x6 -> x4, Pallas kernels: 174 us -> 181 us  [the longest x1 102 us: back(): pl.pallas_call(back_kernel, in_specs=[vmem] * 8, out_specs=vmem, out_shap...]
    gather x2 -> x0, local copies, waits for them, and re-layouts: 7.62 us -> none  [the longest x1 4.95 us: local(): outgoing = padded[slot_table].reshape(experts_all, capacity, features)]
  transfers between devices with their start and end apart: 2 -> 0, of which waited for: 2 -> 0; matrix products, arithmetic and copies ran while one was open for 2% -> 0% of each run, Pallas kernels for 0% -> 0%
where the time goes in v1:
time: 186 us
  Pallas kernels  181 us (97%)
  local copies, waits for them, and re-layouts  4.51 us (2%)
    pallas_call x1, Pallas kernels, back(): pl.pallas_call(back_kernel, in_specs=[vmem] * 8, out_specs=vmem, out_shap...  102 us
    pallas_call x1, Pallas kernels, front(): pl.pallas_call(front_kernel, in_specs=[vmem] * 6, out_specs=vmem, out_sha...  64.7 us
    pallas_call x1, Pallas kernels, mix(): pl.pallas_call(mix_kernel, grid=(pairs,), in_specs=[wide] * 5, out_specs=...  11.8 us
    unnamed x3, local copies, waits for them, and re-layouts  4.51 us

profile of v1, /device:TPU:1, one launch (start us, length us, event | category | flops | bytes accessed | tf_op | source)
XLA Modules:
  0.0 185.7 jit_solution(17152869191097756890)
XLA Ops:
  0.0 1.5 copy.16.ids_ref
  1.5 1.5 copy.17.weight_ref
  2.9 11.8 %mix.1 = (f32[256,512]{1,0:T(8,128)}, bf16[256,128]{1,0:T(8,128)(2,1)}) custom-call(bf16[256,256]{1,0:T(8,128)(2,1)} %r_ref.1, bf16[256,256]{1,0:T(8,128)(2,1)} %k_ref.1, bf16[256,256]{1,0:T(8,128)(2,1)} %v_ref.1, bf16[256,256]{1,0:T(8,128)(2,1)} %d_ref.1, bf16[256,256]{1,0:T(8,128)(2,1)} %a_ref.1), custom_call_target="tpu_custom_call" | custom-call | tf_op jit(solution)/shard_map/mix/pallas_call | solution.py:173
  14.8 64.7 %front.1.mid_ref = bf16[256,256]{1,0:T(8,128)(2,1)} custom-call(f32[256,512]{1,0:T(8,128)} %get-tuple-element.10.reads_ref, bf16[256,128]{1,0:T(8,128)(2,1)} %get-tuple-element.11.states_ref, bf16[256,256]{1,0:T(8,128)(2,1)} %gate_ref.1, f32[1,256]{1,0:T(1,128)} %bitcast.10, bf16[4096,256]{1,0:T(8,128)(2,1)} %weight_ref.2, bf16[256,256]{1,0:T(8,128)(2,1)} %residual_ref.1), custom_call_target="tpu_custom_call" | custom-call | tf_op jit(solution)/shard_map/front/pallas_call | solution.py:451
  79.4 3.0 %route.1 = (bf16[1024,256]{1,0:T(8,128)(2,1)}, bf16[256,1024]{1,0:T(8,128)(2,1)}, bf16[256,1024]{1,0:T(8,128)(2,1)}) custom-call(s32[1]{0:T(128)} %bitcast.2.place_ref, s32[256,2]{1,0:T(8,128)} %copy.16.ids_ref, f32[256,2]{1,0:T(8,128)} %copy.17.weight_ref), custom_call_target="tpu_custom_call" | custom-call | tf_op jit(solution)/shard_map/route/pallas_call | solution.py:217
  82.4 101.7 %back.1 = bf16[256,256]{1,0:T(8,128)(2,1)} custom-call(bf16[256,256]{1,0:T(8,128)(2,1)} %front.1.mid_ref, f32[1,256]{1,0:T(1,128)} %bitcast.9, bf16[1024,256]{1,0:T(8,128)(2,1)} %get-tuple-element.12.pick_ref, bf16[256,1024]{1,0:T(8,128)(2,1)} %get-tuple-element.13.high_ref, bf16[256,1024]{1,0:T(8,128)(2,1)} %get-tuple-element.14.low_ref, ...), custom_call_target="tpu_custom_call" | custom-call | tf_op jit(solution)/shard_map/back/pallas_call | solution.py:682
  184.1 1.6 copy.19

commit v2 on v1

--- a/solution.py
+++ b/solution.py
@@ -1,5 +1,3 @@
-import functools
-
 import jax
 import jax.numpy as jnp
 from jax import lax
@@ -25,10 +23,11 @@
 EPS_NORM = 1e-06
 MESH = pl.DeviceIdType.MESH
 
-OFFSETS = [0]
-for _near in range(1, NZ // 2):
-    OFFSETS += [_near, -_near]
-OFFSETS += [NZ // 2]
+OFFSETS = [NZ // 2]
+for _far in range(NZ // 2 - 1, 0, -1):
+    OFFSETS += [_far, -_far]
+OFFSETS += [0]
+HOME = N_SP - 2
 INVERSE = [OFFSETS.index(-o if o != NZ // 2 else o) for o in OFFSETS]
 
 
@@ -165,69 +164,31 @@
         state_ref[pl.ds(head * HEAD, HEAD), :] = states[head].astype(jnp.bfloat16)
 
 
-def mix(receptance, key_vectors, value_vectors, decay_logits, rate_logits):
-    tokens_here, channels = receptance.shape
-    pairs = channels // (2 * HEAD)
-    wide = pl.BlockSpec((tokens_here, 2 * HEAD), lambda i: (0, i))
-    double = pl.BlockSpec((tokens_here, 4 * HEAD), lambda i: (0, i))
-    return pl.pallas_call(
-        mix_kernel,
-        grid=(pairs,),
-        in_specs=[wide] * 5,
-        out_specs=[double, pl.BlockSpec((2 * HEAD, 2 * HEAD), lambda i: (i, 0))],
-        out_shape=[
-            jax.ShapeDtypeStruct((tokens_here, 2 * channels), jnp.float32),
-            jax.ShapeDtypeStruct((channels, 2 * HEAD), jnp.bfloat16),
-        ],
-        name="mix",
-    )(receptance, key_vectors, value_vectors, decay_logits, rate_logits)
-
-
-def route_kernel(place_ref, ids_ref, weight_ref, pick_ref, high_ref, low_ref):
-    tokens = ids_ref.shape[0]
+def route(place, ids_ref, weight_ref, pick_ref, high_ref, low_ref):
+    tokens = ids_ref.shape[1]
     slots = N_SP * CAP
-    expert = lax.broadcasted_iota(jnp.int32, (tokens, 128), 1)
-    named = [ids_ref[:, k : k + 1] == expert for k in range(2)]
+    expert = lax.broadcasted_iota(jnp.int32, (128, tokens), 0)
+    named = [ids_ref[k : k + 1, :] == expert for k in range(2)]
     onehot = jnp.where(named[0] | named[1], 1.0, 0.0).astype(jnp.bfloat16)
     row = lax.broadcasted_iota(jnp.int32, (tokens, tokens), 0)
     col = lax.broadcasted_iota(jnp.int32, (tokens, tokens), 1)
-    before = jnp.where(col < row, 1.0, 0.0).astype(jnp.bfloat16)
-    earlier = dot(before, onehot, NN).astype(jnp.bfloat16)
-    weight = jnp.where(named[0], weight_ref[:, 0:1], 0.0) + jnp.where(named[1], weight_ref[:, 1:2], 0.0)
+    before = jnp.where(row < col, 1.0, 0.0).astype(jnp.bfloat16)
+    earlier = dot(onehot, before, NN).astype(jnp.bfloat16)
+    weight = jnp.where(named[0], weight_ref[0:1, :], 0.0) + jnp.where(named[1], weight_ref[1:2, :], 0.0)
     high, low = split(weight)
-    slot = lax.broadcasted_iota(jnp.int32, (128, slots), 1)
-    source = lax.broadcasted_iota(jnp.int32, (128, slots), 0)
+    slot = lax.broadcasted_iota(jnp.int32, (slots, 128), 0)
+    source = lax.broadcasted_iota(jnp.int32, (slots, 128), 1)
     near = slot // (2 * CAP)
-    step = (near + 1) // 2
+    step = NZ // 2 - (near + 1) // 2
     off = jnp.where(near % 2 == 1, step, NZ - step)
-    chip = (place_ref[0] // 2 + off) % NZ
-    core = (place_ref[0] + slot // CAP) % 2
+    chip = (place.z + off) % NZ
+    core = (place.core + slot // CAP) % 2
     spread = jnp.where(source == chip * 2 + core, 1.0, 0.0).astype(jnp.bfloat16)
-    rank = (lax.broadcasted_iota(jnp.int32, (tokens, slots), 1) % CAP).astype(jnp.float32)
-    taken = jnp.where(dot(earlier, spread, NN) == rank, dot(onehot, spread, NN), 0.0)
-    pick_ref[...] = taken.T.astype(jnp.bfloat16)
-    high_ref[...] = (taken * dot(high, spread, NN)).astype(jnp.bfloat16)
-    low_ref[...] = (taken * dot(low, spread, NN)).astype(jnp.bfloat16)
-
-
-def route(expert_ids, route_weight):
-    tokens = expert_ids.shape[0]
-    slots = N_SP * CAP
-    place = lax.axis_index("sp").astype(jnp.int32).reshape(1)
-    return pl.pallas_call(
-        route_kernel,
-        in_specs=[
-            pl.BlockSpec(memory_space=pltpu.SMEM),
-            pl.BlockSpec(memory_space=pltpu.VMEM),
-            pl.BlockSpec(memory_space=pltpu.VMEM),
-        ],
-        out_shape=[
-            jax.ShapeDtypeStruct((slots, tokens), jnp.bfloat16),
-            jax.ShapeDtypeStruct((tokens, slots), jnp.bfloat16),
-            jax.ShapeDtypeStruct((tokens, slots), jnp.bfloat16),
-        ],
-        name="route",
-    )(place, expert_ids, route_weight)
+    rank = (lax.broadcasted_iota(jnp.int32, (slots, tokens), 0) % CAP).astype(jnp.float32)
+    taken = jnp.where(dot(spread, earlier, NN) == rank, dot(spread, onehot, NN), 0.0)
+    pick_ref[...] = taken.astype(jnp.bfloat16)
+    high_ref[...] = (taken * dot(spread, high, NN)).astype(jnp.bfloat16)
+    low_ref[...] = (taken * dot(spread, low, NN)).astype(jnp.bfloat16)
 
 
 class Place:
@@ -276,13 +237,6 @@
             copy.wait_send()
 
 
-def greet(devices):
-    barrier = pltpu.get_barrier_semaphore()
-    for device in devices:
-        pl.semaphore_signal(barrier, inc=1, device_id=device, device_id_type=MESH)
-    return lambda: pl.semaphore_wait(barrier, len(devices))
-
-
 ORDER = (("x", "y"), ("y", "x"))
 
 
@@ -323,14 +277,14 @@
             return block.at[pl.ds(place.on(second, off) * SIDE, SIDE)]
 
         if n == 0:
-            s["a"] = self.exchange(h, first, one)
+            s["a"] = [self.copies(one(0), one(0), place.along(first, off)) for off in (2, 1, -1)]
+            for copy in s["a"]:
+                copy.start()
         elif n == 1:
-            s["b"] = self.relay(*s["a"], one, lambda ref, side: ref.at[side])
-        elif n == 2:
-            for copy in s["b"]:
+            for copy in s["a"]:
                 copy.wait_recv()
             s["c"] = self.exchange(h, second, four)
-        elif n == 3:
+        elif n == 2:
             s["d"] = self.relay(*s["c"], four, lambda ref, side: ref.at[:, side])
         else:
             for copy in s["d"]:
@@ -343,21 +297,16 @@
     return [x * SIDE + y for y in range(SIDE) for x in range(SIDE)]
 
 
-def front_kernel(
-    reads_ref, states_ref, gate_ref, gain_ref, weight_ref, residual_ref,
-    out_ref, maps, half_a, half_b, send, recv,
+def front(
+    place, copies, meanwhile,
+    reads_ref, states_ref, gate_ref, gain_ref, weight_ref, residual_ref, out_ref, maps, halves,
 ):
-    place = Place()
-    copies = Copies(send, recv)
     partner = place.at_z(0, True)
     up, down = place.at_z(1), place.at_z(-1)
-    neighbours = [partner, up, down] + [place.along(axis, off) for axis in "xy" for off in (1, -1)]
-    wait = greet(neighbours)
     tokens = out_ref.shape[0]
     pieces = 2
     rows = states_ref.shape[0] // pieces
     maps[place.sp] = states_ref[...]
-    wait()
 
     def slot(off):
         return place.chip(off)
@@ -378,6 +327,7 @@
         for direction in (1, -1):
             current[direction, piece] = hop(1, direction, piece)
     across[0].start()
+    meanwhile()
     for n in range(1, NZ // 2 + 1):
         for piece in range(pieces):
             for direction in (1, -1):
@@ -422,14 +372,13 @@
         * gain_ref[...]
         * sigmoid(gate_ref[...].astype(jnp.float32))
     ).astype(jnp.bfloat16)
-    halves = (half_a, half_b)
     gather = TorusGather(place, copies, halves)
     quarter = tokens // 4
     for h in range(2):
         for q in range(2):
             at = (2 * h + q) * quarter
             halves[h][gather.own(h), q] = gated[at : at + quarter]
-    for n in range(5):
+    for n in range(4):
         for h in range(2):
             gather.stage(n, h)
     width = gated.shape[1]
@@ -440,29 +389,6 @@
             total += dot(block, weight_ref[pl.ds(t * width, width), :], NN)
         part = pl.ds(h * (tokens // 2), tokens // 2)
         out_ref[part, :] = (residual_ref[part, :].astype(jnp.float32) + total).astype(jnp.bfloat16)
-    copies.drain()
-
-
-def front(reads, states, gate_logits, group_gain, mixer_out, residual):
-    tokens, channels = gate_logits.shape
-    quarter = tokens // 4
-    count = 64
-    vmem = pl.BlockSpec(memory_space=pltpu.VMEM)
-    return pl.pallas_call(
-        front_kernel,
-        in_specs=[vmem] * 6,
-        out_specs=vmem,
-        out_shape=jax.ShapeDtypeStruct(residual.shape, jnp.bfloat16),
-        scratch_shapes=[
-            pltpu.VMEM((N_SP, *states.shape), jnp.bfloat16),
-            pltpu.VMEM((N_TP, 2, quarter, channels), jnp.bfloat16),
-            pltpu.VMEM((N_TP, 2, quarter, channels), jnp.bfloat16),
-            pltpu.SemaphoreType.DMA((count,)),
-            pltpu.SemaphoreType.DMA((count,)),
-        ],
-        compiler_params=pltpu.CompilerParams(collective_id=0, has_side_effects=True),
-        name="front",
-    )(reads, states, gate_logits, group_gain.reshape(1, channels), mixer_out, residual)
 
 
 EXTRA = 128
@@ -483,48 +409,42 @@
                 pltpu.VMEM((PARTS, SIDE, SUB, w), jnp.bfloat16),
                 pltpu.VMEM((PARTS, 2, SIDE, SUB, w), jnp.bfloat16),
                 pltpu.VMEM((PARTS, SIDE, SUB, w), jnp.bfloat16),
-                pltpu.VMEM((PARTS, SUB, w), jnp.bfloat16),
-                pltpu.VMEM((PARTS, 2, SUB, w), jnp.bfloat16),
+                pltpu.VMEM((PARTS, 3, SUB, w), jnp.bfloat16),
             ]
     hidden = [pltpu.VMEM((PARTS, N_TP, 2, SUB, ff // 4), jnp.bfloat16) for _ in range(2)]
     slots = [pltpu.VMEM((N_SP, CAP, features), jnp.bfloat16) for _ in range(4)]
-    count = 2 * (N_SP - 1) + PARTS * (24 + 16)
-    return slots + hidden + per_part + [
-        pltpu.SemaphoreType.DMA((count,)),
-        pltpu.SemaphoreType.DMA((count,)),
-    ]
+    return slots + hidden + per_part
 
 
 REDUCE = (("y", "x"), ("x", "y"))
 
 
-def back_kernel(
-    mid_ref, gain_ref, pick_ref, high_ref, low_ref, gate_ref, up_ref, down_ref, out_ref, *scratch
-):
-    outgoing, arrived, results, returned = scratch[:4]
-    hidden = scratch[4:6]
-    buffers = [[scratch[6 + (2 * h + q) * 6 : 12 + (2 * h + q) * 6] for q in range(2)] for h in range(2)]
-    send, recv = scratch[30:]
-    place = Place()
-    copies = Copies(send, recv)
-    features = mid_ref.shape[1]
-    ff = gate_ref.shape[1]
-    half = ff // 2
-    z_peers = [
+def peers_along_z(place):
+    return [
         (2 * near + other, 2 * INVERSE[near] + other, place.at_z(off, bool(other)))
         for near, off in enumerate(OFFSETS)
         for other in range(2)
         if off != 0 or other
     ]
-    ring = [place.along(axis, off) for axis in "xy" for off in (1, -1)]
-    wait = greet([peer[2] for peer in z_peers] + ring)
+
+
+def back(
+    place, copies,
+    mid_ref, gain_ref, pick_ref, high_ref, low_ref, gate_ref, up_ref, down_ref, out_ref, scratch,
+):
+    outgoing, arrived, results, returned = scratch[:4]
+    hidden = scratch[4:6]
+    buffers = [[scratch[6 + (2 * h + q) * 5 : 11 + (2 * h + q) * 5] for q in range(2)] for h in range(2)]
+    features = mid_ref.shape[1]
+    ff = gate_ref.shape[1]
+    half = ff // 2
+    z_peers = peers_along_z(place)
     for part in range(PARTS):
         rows = pl.ds(part * POS * CAP, POS * CAP)
         outgoing[pl.ds(part * POS, POS)] = (
             dot(pick_ref[rows, :], mid_ref[...], NN).astype(jnp.bfloat16).reshape(POS, CAP, features)
         )
-    arrived[0] = outgoing[0]
-    wait()
+    arrived[HOME] = outgoing[HOME]
     dispatch = {}
     for at, there, device in z_peers:
         dispatch[at] = copies(outgoing.at[at], arrived.at[there], device)
@@ -542,56 +462,60 @@
             total += ref.astype(jnp.float32)
         return total
 
-    def relay_out(part, h, level):
-        axis = REDUCE[h][level]
-        far = place.on(axis, 2)
+    def relay_out(part, h):
+        axis = REDUCE[h][0]
+        far = pl.ds(place.on(axis, 2) * SIDE, SIDE)
         sent = []
         for q, off in ((0, 1), (1, -1)):
-            product, passed1, _, reduced, passed2, _ = buffers[h][q]
-            if level == 0:
-                src, dst = product.at[part, pl.ds(far * SIDE, SIDE)], passed1.at[part]
-            else:
-                src, dst = reduced.at[part, far], passed2.at[part]
-            copy = copies(src, dst, place.along(axis, off))
+            product, passed = buffers[h][q][:2]
+            copy = copies(product.at[part, far], passed.at[part], place.along(axis, off))
             copy.start()
             sent.append(copy)
-        state[part][h, level, "relay"] = sent
-
-    def join(part, h, level):
-        axis = REDUCE[h][level]
+        state[part][h, "relay"] = sent
+
+    def join(part, h):
+        axis = REDUCE[h][0]
         sent = []
         for side, off in ((0, 1), (1, -1)):
-            state[part][h, level, "relay"][side].wait_recv()
-            near = place.on(axis, off)
-            for q in (side, 1 - side):
-                product, passed1, both1, reduced, passed2, both2 = buffers[h][q]
-                if level == 0:
-                    at, mine, dst = pl.ds(near * SIDE, SIDE), product, both1.at[part, side]
-                    other = passed1
-                else:
-                    at, mine, dst = near, reduced, both2.at[part, side]
-                    other = passed2
+            state[part][h, "relay"][side].wait_recv()
+            near = pl.ds(place.on(axis, off) * SIDE, SIDE)
+            for q in (1 - side, side):
+                product, passed, both = buffers[h][q][:3]
                 if q == side:
-                    mine[part, at] = add(mine[part, at], other[part]).astype(jnp.bfloat16)
-                copy = copies(mine.at[part, at], dst, place.along(axis, off))
+                    product[part, near] = add(product[part, near], passed[part]).astype(jnp.bfloat16)
+                copy = copies(product.at[part, near], both.at[part, side], place.along(axis, off))
                 copy.start()
                 sent.append(copy)
-        state[part][h, level, "both"] = sent
-
-    def finish(part, h, level):
-        axis = REDUCE[h][level]
-        for copy in state[part][h, level, "both"]:
+        state[part][h, "both"] = sent
+
+    def halfway(part, h):
+        first, second = REDUCE[h]
+        for copy in state[part][h, "both"]:
             copy.wait_recv()
-        here = place.on(axis)
-        totals = []
+        here = pl.ds(place.on(first) * SIDE, SIDE)
+        sent = []
         for q in range(2):
-            product, _, both1, reduced, _, both2 = buffers[h][q]
-            if level == 0:
-                total = add(product[part, pl.ds(here * SIDE, SIDE)], both1[part, 0], both1[part, 1])
-                reduced[part] = total.astype(jnp.bfloat16)
-            else:
-                totals.append(add(reduced[part, here], both2[part, 0], both2[part, 1]))
-        return totals
+            product, _, both, reduced, others = buffers[h][q]
+            total = add(product[part, here], both[part, 0], both[part, 1])
+            reduced[part] = total.astype(jnp.bfloat16)
+            for side, off in enumerate((2, 1, -1)):
+                copy = copies(
+                    reduced.at[part, place.on(second, off)],
+                    others.at[part, side],
+                    place.along(second, off),
+                )
+                copy.start()
+                sent.append(copy)
+        state[part][h, "others"] = sent
+
+    def finish(part, h):
+        second = REDUCE[h][1]
+        for copy in state[part][h, "others"]:
+            copy.wait_recv()
+        return [
+            add(reduced[part, place.on(second)], *[others[part, side] for side in range(3)])
+            for _, _, _, reduced, others in buffers[h]
+        ]
 
     def products(part):
         for at in range(part * POS, (part + 1) * POS):
@@ -610,10 +534,10 @@
                     product[part, at, :, pl.ds(0, half)] = value[t]
                     if h == 0 and q == 0:
                         product[part, at, :, pl.ds(half, EXTRA)] = extra[t * SUB : (t + 1) * SUB]
-            relay_out(part, h, 0)
+            relay_out(part, h)
 
     def activate(part):
-        (gate_a, up_a), (gate_b, up_b) = [finish(part, h, 1) for h in range(2)]
+        (gate_a, up_a), (gate_b, up_b) = [finish(part, h) for h in range(2)]
         inv = lax.rsqrt(gate_a[:, half : half + 1] * (1.0 / D) + EPS_NORM)
         gather = gathers[part]
         for h, (gate, up) in enumerate(((gate_a[:, :half], up_a), (gate_b, up_b))):
@@ -626,7 +550,7 @@
     def outputs(part):
         total = jnp.zeros((POS * CAP, features), jnp.float32)
         for h in range(2):
-            gathers[part].stage(4, h)
+            gathers[part].stage(3, h)
             for q in range(2):
                 blocks = [hidden[h][part, at, q] for at in torus_order(h)]
                 at = h * half + q * (half // 2)
@@ -636,8 +560,8 @@
             if part * POS <= at < (part + 1) * POS:
                 back[at] = copies(results.at[at], returned.at[there], device)
                 back[at].start()
-        if part == 0:
-            returned[0] = results[0]
+        if part == HOME // POS:
+            returned[HOME] = results[HOME]
 
     def both(action):
         def run(part):
@@ -647,16 +571,14 @@
 
     stages = [
         products,
-        both(lambda part, h: join(part, h, 0)),
-        both(lambda part, h: (finish(part, h, 0), relay_out(part, h, 1))),
-        both(lambda part, h: join(part, h, 1)),
+        both(join),
+        both(halfway),
         activate,
         both(lambda part, h: gathers[part].stage(1, h)),
         both(lambda part, h: gathers[part].stage(2, h)),
-        both(lambda part, h: gathers[part].stage(3, h)),
         outputs,
     ]
-    begins = (0.0, 5.0, 12.0, 21.0)
+    begins = (0.0, 7.0, 11.0, 13.0)
     plan = sorted(
         (begins[part] + 3.0 * n, part, n) for part in range(PARTS) for n in range(len(stages))
     )
@@ -671,23 +593,55 @@
                 came[at].wait_recv()
         rows = returned[pl.ds(part * POS, POS)].reshape(POS * CAP, features)
         columns = pl.ds(part * POS * CAP, POS * CAP)
-        total += dot(high_ref[:, columns], rows, NN) + dot(low_ref[:, columns], rows, NN)
+        total += dot(high_ref[columns, :], rows, TN) + dot(low_ref[columns, :], rows, TN)
     out_ref[...] = total.astype(jnp.bfloat16)
+
+
+def kernel(
+    r_ref, k_ref, v_ref, d_ref, a_ref, gate_logits_ref, group_gain_ref, residual_ref, norm_gain_ref,
+    ids_ref, route_weight_ref, mixer_hbm, gate_hbm, up_hbm, down_hbm, out_ref, *scratch
+):
+    mixer, gate, up, down, loaded, send, recv = scratch[:7]
+    reads, states, pick, high, low, midway, maps = scratch[7:14]
+    halves = scratch[14:16]
+    place = Place()
+    copies = Copies(send, recv)
+    barrier = pltpu.get_barrier_semaphore()
+    others = [peer[2] for peer in peers_along_z(place)]
+    others += [place.along(axis, off) for axis in "xy" for off in (2, 1, -1)]
+    for device in others:
+        pl.semaphore_signal(barrier, inc=1, device_id=device, device_id_type=MESH)
+    loads = [
+        pltpu.make_async_copy(src, dst, loaded.at[n])
+        for n, (src, dst) in enumerate(
+            [(mixer_hbm, mixer), (gate_hbm, gate), (up_hbm, up), (down_hbm, down)]
+        )
+    ]
+    for load in loads:
+        load.start()
+    for pair in range(r_ref.shape[1] // (2 * HEAD)):
+        lanes = pl.ds(pair * 2 * HEAD, 2 * HEAD)
+        mix_kernel(
+            *[ref.at[:, lanes] for ref in (r_ref, k_ref, v_ref, d_ref, a_ref)],
+            reads.at[:, pl.ds(pair * 4 * HEAD, 4 * HEAD)],
+            states.at[lanes, :],
+        )
+    pl.semaphore_wait(barrier, len(others))
+
+    def meanwhile():
+        route(place, ids_ref, route_weight_ref, pick, high, low)
+        for load in loads:
+            load.wait()
+
+    front(
+        place, copies, meanwhile,
+        reads, states, gate_logits_ref, group_gain_ref, mixer, residual_ref, midway, maps, halves,
+    )
+    back(
+        place, copies,
+        midway, norm_gain_ref, pick, high, low, gate, up, down, out_ref, scratch[16:],
+    )
     copies.drain()
-
-
-def back(midway, norm_gain, pick, high, low, gate, up, down):
-    features = midway.shape[1]
-    vmem = pl.BlockSpec(memory_space=pltpu.VMEM)
-    return pl.pallas_call(
-        back_kernel,
-        in_specs=[vmem] * 8,
-        out_specs=vmem,
-        out_shape=jax.ShapeDtypeStruct(midway.shape, jnp.bfloat16),
-        scratch_shapes=back_scratch(gate.shape[1], features),
-        compiler_params=pltpu.CompilerParams(collective_id=1, has_side_effects=True),
-        name="back",
-    )(midway, norm_gain.reshape(1, features), pick, high, low, gate, up, down)
 
 
 def local(
@@ -707,10 +661,45 @@
     expert_up,
     expert_down,
 ):
-    reads, states = mix(receptance, key_vectors, value_vectors, decay_logits, rate_logits)
-    pick, high, low = route(expert_ids, route_weight)
-    midway = front(reads, states, gate_logits, group_gain, mixer_out, residual)
-    return back(midway, norm_gain, pick, high, low, expert_gate[0], expert_up[0], expert_down[0])
+    tokens, channels = residual.shape
+    features = norm_gain.shape[0]
+    ff = expert_gate.shape[2]
+    slots = N_SP * CAP
+    count = 64 + 2 * (N_SP - 1) + PARTS * 40
+    bf16 = jnp.bfloat16
+    vmem = pl.BlockSpec(memory_space=pltpu.VMEM)
+    hbm = pl.BlockSpec(memory_space=pl.ANY)
+    weights = (mixer_out, expert_gate[0], expert_up[0], expert_down[0])
+    return pl.pallas_call(
+        kernel,
+        in_specs=[vmem] * 11 + [hbm] * 4,
+        out_specs=vmem,
+        out_shape=jax.ShapeDtypeStruct((tokens, features), bf16),
+        scratch_shapes=[pltpu.VMEM(w.shape, bf16) for w in weights]
+        + [
+            pltpu.SemaphoreType.DMA((len(weights),)),
+            pltpu.SemaphoreType.DMA((count,)),
+            pltpu.SemaphoreType.DMA((count,)),
+            pltpu.VMEM((tokens, 2 * channels), jnp.float32),
+            pltpu.VMEM((channels, 2 * HEAD), bf16),
+            pltpu.VMEM((slots, tokens), bf16),
+            pltpu.VMEM((slots, tokens), bf16),
+            pltpu.VMEM((slots, tokens), bf16),
+            pltpu.VMEM((tokens, features), bf16),
+            pltpu.VMEM((N_SP, channels, 2 * HEAD), bf16),
+            pltpu.VMEM((N_TP, 2, tokens // 4, channels), bf16),
+            pltpu.VMEM((N_TP, 2, tokens // 4, channels), bf16),
+        ]
+        + back_scratch(ff, features),
+        compiler_params=pltpu.CompilerParams(
+            collective_id=0, has_side_effects=True, vmem_limit_bytes=60 * 1024 * 1024
+        ),
+        name="layer",
+    )(
+        receptance, key_vectors, value_vectors, decay_logits, rate_logits, gate_logits,
+        group_gain.reshape(1, channels), residual, norm_gain.reshape(1, features),
+        expert_ids.T, route_weight.T, *weights,
+    )
 
 
 def solution(mesh):

time: 186 us -> 158 us (0.85)
  Pallas kernels: 181 us -> 157 us
  local copies, waits for them, and re-layouts: 4.51 us -> 1.57 us
    pallas_call x4 -> x1, Pallas kernels: 181 us -> 157 us  [local(): pl.pallas_call(kernel, in_specs=[vmem] * 11 + [hbm] * 4, out_specs=vmem,...]
    unnamed x3 -> x1, local copies, waits for them, and re-layouts: 4.51 us -> 1.57 us
where the time goes in v2:
time: 158 us
  Pallas kernels  157 us (99%)
    pallas_call x1, Pallas kernels, local(): pl.pallas_call(kernel, in_specs=[vmem] * 11 + [hbm] * 4, out_specs=vmem,...  157 us

profile of v2, /device:TPU:1, one launch (start us, length us, event | category | flops | bytes accessed | tf_op | source)
XLA Modules:
  0.0 158.2 jit_solution(3014610317017225720)
XLA Ops:
  0.0 156.6 %layer.1 = bf16[256,256]{1,0:T(8,128)(2,1)} custom-call(bf16[256,256]{1,0:T(8,128)(2,1)} %r_ref.1, bf16[256,256]{1,0:T(8,128)(2,1)} %k_ref.1, bf16[256,256]{1,0:T(8,128)(2,1)} %v_ref.1, bf16[256,256]{1,0:T(8,128)(2,1)} %d_ref.1, bf16[256,256]{1,0:T(8,128)(2,1)} %a_ref.1, bf16[256,256]{1,0:T(8,128)(2,1)} %gate_logits_ref.1, f32[1,256]{1,0:T(1,128)} %bitcast.12, ...), custom_call_target="tpu_custom_call" | custom-call | tf_op jit(solution)/shard_map/layer/pallas_call | solution.py:673
  156.7 1.6 copy.17

commit v3 on v2

--- a/solution.py
+++ b/solution.py
@@ -17,7 +17,7 @@
 CAP = 32
 PARTS = 4
 POS = N_SP // PARTS
-SUB = POS * CAP // N_TP
+SUB = POS * CAP // 8
 
 EPS_GROUP = 0.00064
 EPS_NORM = 1e-06
@@ -245,111 +245,90 @@
         self.place, self.copies, self.blocks = place, copies, blocks
         self.state = [dict() for _ in blocks]
 
-    def own(self, h):
-        first, second = ORDER[h]
-        return self.place.on(second) * SIDE + self.place.on(first)
-
-    def exchange(self, h, axis, mine):
-        up, down = self.place.along(axis, 1), self.place.along(axis, -1)
-        whole = mine(0)
-        direct = [self.copies(whole, whole, up), self.copies(whole, whole, down)]
-        for copy in direct:
+    def at(self, h, first=0, second=0):
+        one, two = ORDER[h]
+        return self.place.on(two, second) * SIDE + self.place.on(one, first)
+
+    def block(self, h, first=0, second=0):
+        return self.blocks[h].at[self.at(h, first, second)]
+
+    def row(self, h, second=0):
+        start = self.place.on(ORDER[h][1], second) * SIDE
+        return self.blocks[h].at[pl.ds(start, SIDE)]
+
+    def begin(self, h):
+        mine = self.block(h)
+        sent = {off: self.copies(mine, mine, self.place.along(ORDER[h][0], off)) for off in (2, 1, -1)}
+        for copy in sent.values():
             copy.start()
-        return direct, up, down
-
-    def relay(self, direct, up, down, mine, half):
+        self.state[h]["first"] = sent
+
+    def arrive(self, h, off):
+        self.state[h]["first"][off].wait_recv()
+
+    def pair(self, h, ref):
+        sent = [self.copies(ref, ref, self.place.along(ORDER[h][1], off)) for off in (1, -1)]
+        for copy in sent:
+            copy.start()
+        return sent
+
+    def relay(self, h, sent, ref_of, half):
         passed = []
-        for side, (copy, off, target) in enumerate(zip(direct, (-1, 1), (up, down))):
+        for side, (copy, off) in enumerate(zip(sent, (1, -1))):
             copy.wait_recv()
-            piece = half(mine(off), side)
-            passed.append(self.copies(piece, piece, target))
+            piece = half(ref_of(-off), side)
+            passed.append(self.copies(piece, piece, self.place.along(ORDER[h][1], off)))
             passed[-1].start()
         return passed
 
-    def stage(self, n, h):
-        first, second = ORDER[h]
-        place, block, s = self.place, self.blocks[h], self.state[h]
-
-        def one(off):
-            return block.at[place.on(second) * SIDE + place.on(first, off)]
-
-        def four(off):
-            return block.at[pl.ds(place.on(second, off) * SIDE, SIDE)]
-
-        if n == 0:
-            s["a"] = [self.copies(one(0), one(0), place.along(first, off)) for off in (2, 1, -1)]
-            for copy in s["a"]:
-                copy.start()
-        elif n == 1:
-            for copy in s["a"]:
-                copy.wait_recv()
-            s["c"] = self.exchange(h, second, four)
-        elif n == 2:
-            s["d"] = self.relay(*s["c"], four, lambda ref, side: ref.at[:, side])
-        else:
-            for copy in s["d"]:
-                copy.wait_recv()
-
-
-def torus_order(h):
-    if h == 0:
-        return list(range(N_TP))
-    return [x * SIDE + y for y in range(SIDE) for x in range(SIDE)]
-
 
 def front(
     place, copies, meanwhile,
-    reads_ref, states_ref, gate_ref, gain_ref, weight_ref, residual_ref, out_ref, maps, halves,
+    reads_ref, states_ref, gate_ref, gain_ref, weight_ref, residual_ref, out_ref,
+    cores, maps, incoming_ref, halves,
 ):
     partner = place.at_z(0, True)
-    up, down = place.at_z(1), place.at_z(-1)
     tokens = out_ref.shape[0]
-    pieces = 2
-    rows = states_ref.shape[0] // pieces
-    maps[place.sp] = states_ref[...]
-
-    def slot(off):
-        return place.chip(off)
-
-    def hop(n, direction, piece):
-        part = pl.ds(piece * rows, rows)
-        target = up if direction > 0 else down
-        here = slot(-direction * (n - 1))
-        src = states_ref.at[part] if n == 1 else maps.at[here, part]
-        copy = copies(src, maps.at[here, part], target)
-        copy.start()
-        return copy
-
-    across = [copies(states_ref, maps.at[slot(0)], partner)]
+    heads = states_ref.shape[0] // HEAD
+    mine = heads // 2
+    cores[place.core] = states_ref[...]
+    swap = copies(states_ref, cores.at[place.core], partner)
+    swap.start()
+    swap.wait_recv()
+    for head in range(mine):
+        rows = pl.ds(pl.multiple_of((place.core * mine + head) * HEAD, HEAD), HEAD)
+        later = cores[1, rows, :]
+        added = dot(later[:, HEAD:], cores[0, rows, :], NN)
+        state = later[:, :HEAD].astype(jnp.float32) + added[:, :HEAD]
+        maps[place.z, pl.ds(head * HEAD, HEAD), :] = jnp.concatenate(
+            [state, added[:, HEAD:]], axis=1
+        ).astype(jnp.bfloat16)
+
+    came = {}
     last = {1: NZ // 2, -1: NZ // 2 - 1}
-    current = {}
-    for piece in range(pieces):
+
+    def pass_on(direction, d):
+        ref = maps.at[(place.z - direction * d + NZ) % NZ]
+        for far in (2, 1):
+            if d + far <= last[direction]:
+                came[direction, d + far] = copies(ref, ref, place.at_z(direction * far))
+                came[direction, d + far].start()
+
+    for d in range(0, NZ // 2, 2):
         for direction in (1, -1):
-            current[direction, piece] = hop(1, direction, piece)
-    across[0].start()
-    meanwhile()
-    for n in range(1, NZ // 2 + 1):
-        for piece in range(pieces):
-            for direction in (1, -1):
-                if n > last[direction]:
-                    continue
-                current[direction, piece].wait_recv()
-                if n < last[direction]:
-                    current[direction, piece] = hop(n + 1, direction, piece)
-        for direction in (1, -1):
-            if n <= last[direction]:
-                here = slot(-direction * n)
-                copy = copies(maps.at[here], maps.at[here], partner)
-                copy.start()
-                across.append(copy)
-    for copy in across:
-        copy.wait_recv()
-
-    heads = states_ref.shape[0] // HEAD
+            if d:
+                came[direction, d].wait_recv()
+            pass_on(direction, d)
+        if d // 2 < len(meanwhile):
+            meanwhile[d // 2]()
+    for direction in (1, -1):
+        for d in range(1, last[direction] + 1):
+            if d % 2 or d == NZ // 2:
+                came[direction, d].wait_recv()
 
     def fold(step, carried):
         following = []
-        for head in range(heads):
+        for head in range(mine):
             both = maps[step, pl.ds(head * HEAD, HEAD), :]
             hi, lo = split(carried[head])
             step_map = both[:, HEAD:]
@@ -359,11 +338,23 @@
         return tuple(following)
 
     zero = jnp.zeros((HEAD, HEAD), jnp.float32)
-    incoming = lax.fori_loop(0, place.sp, fold, (zero,) * heads)
+    incoming_ref[place.core] = jnp.concatenate(
+        lax.fori_loop(0, place.z, fold, (zero,) * mine), axis=1
+    )
+    swap = copies(incoming_ref.at[place.core], incoming_ref.at[place.core], partner)
+    swap.start()
+    second = (jnp.zeros((HEAD, HEAD), jnp.int32) + place.core) == 1
+    swap.wait_recv()
     scaled = []
     for head in range(heads):
+        before = incoming_ref[head // mine, :, (head % mine) * HEAD : (head % mine + 1) * HEAD]
+        both = cores[0, pl.ds(head * HEAD, HEAD), :]
+        hi, lo = split(before)
+        step_map = both[:, HEAD:]
+        after = both[:, :HEAD].astype(jnp.float32) + dot(step_map, hi, NN) + dot(step_map, lo, NN)
+        state = jnp.where(second, after, before)
         both = reads_ref[:, pl.ds(head * 2 * HEAD, 2 * HEAD)]
-        state_read = both[:, :HEAD] + dot3(split(both[:, HEAD:]), split(incoming[head]))
+        state_read = both[:, :HEAD] + dot3(split(both[:, HEAD:]), split(state))
         centred = state_read - jnp.mean(state_read, axis=1, keepdims=True)
         variance = jnp.mean(centred * centred, axis=1, keepdims=True)
         scaled.append(centred * lax.rsqrt(variance + EPS_GROUP))
@@ -377,46 +368,86 @@
     for h in range(2):
         for q in range(2):
             at = (2 * h + q) * quarter
-            halves[h][gather.own(h), q] = gated[at : at + quarter]
-    for n in range(4):
+            halves[h][gather.at(h), q] = gated[at : at + quarter]
+    width = gated.shape[1]
+    totals = [jnp.zeros((tokens // 2, out_ref.shape[1]), jnp.float32) for _ in range(2)]
+
+    def project(h, first, second):
+        x, y = (first, second) if h == 0 else (second, first)
+        t = place.on("y", y) * SIDE + place.on("x", x)
+        rows = pl.ds(pl.multiple_of(t * width, width), width)
+        block = halves[h][gather.at(h, first, second)].reshape(tokens // 2, width)
+        totals[h] += dot(block, weight_ref[rows, :], NN)
+
+    pairs, passed = {}, {}
+    for h in range(2):
+        gather.begin(h)
+    for h in range(2):
+        pairs[h, 0] = gather.pair(h, gather.block(h))
+    for off in (1, -1, 2):
         for h in range(2):
-            gather.stage(n, h)
-    width = gated.shape[1]
+            gather.arrive(h, off)
+            pairs[h, -off] = gather.pair(h, gather.block(h, -off))
+    for first in (0, -1, 1, -2):
+        for h in range(2):
+            passed[h, first] = gather.relay(
+                h, pairs[h, first],
+                lambda second, h=h, first=first: gather.block(h, first, second),
+                lambda ref, side: ref.at[side],
+            )
+        for h in range(2):
+            project(h, first, 0)
+            project(h, first, 1)
+            project(h, first, -1)
+    for first in (0, -1, 1, -2):
+        for h in range(2):
+            for copy in passed[h, first]:
+                copy.wait_recv()
+            project(h, first, 2)
     for h in range(2):
-        total = jnp.zeros((tokens // 2, out_ref.shape[1]), jnp.float32)
-        for t, at in enumerate(torus_order(h)):
-            block = halves[h][at].reshape(tokens // 2, width)
-            total += dot(block, weight_ref[pl.ds(t * width, width), :], NN)
         part = pl.ds(h * (tokens // 2), tokens // 2)
-        out_ref[part, :] = (residual_ref[part, :].astype(jnp.float32) + total).astype(jnp.bfloat16)
+        out_ref[part, :] = (residual_ref[part, :].astype(jnp.float32) + totals[h]).astype(jnp.bfloat16)
 
 
 EXTRA = 128
-
-
-def widths(ff):
-    return ((ff // 2 + EXTRA, ff // 2), (ff // 2, ff // 2))
+SPREAD = ("y", "x")
+SUM = ("x", "y")
 
 
 def back_scratch(ff, features):
-    wide = widths(ff)
-    per_part = []
+    quarter = ff // SIDE
+    scratch = [pltpu.VMEM((N_SP, CAP, features), jnp.bfloat16) for _ in range(3)]
+    for _ in range(2):
+        scratch += [
+            pltpu.VMEM((SIDE, features, 2 * quarter), jnp.bfloat16),
+            pltpu.VMEM((PARTS, SIDE, 2, POS // 4 * CAP, features), jnp.bfloat16),
+            pltpu.VMEM((PARTS, SIDE, SUB, 2 * quarter + EXTRA), jnp.bfloat16),
+            pltpu.VMEM((PARTS, 3, SUB, 2 * quarter + EXTRA), jnp.bfloat16),
+            pltpu.VMEM((PARTS, N_TP, 2, SUB // 2, quarter), jnp.bfloat16),
+        ]
+    return scratch
+
+
+def spread_weights(place, copies, gain_ref, gate, up, scratch):
+    gain = jnp.broadcast_to(gain_ref[...], (128, gain_ref.shape[1])).T[:, :1]
+    quarter = gate.shape[1] // SIDE
+    for matrix in (gate, up):
+        matrix[...] = (matrix[...].astype(jnp.float32) * gain).astype(jnp.bfloat16)
+    sent = []
     for h in range(2):
-        for q in range(2):
-            w = wide[h][q]
-            per_part += [
-                pltpu.VMEM((PARTS, N_TP, SUB, w), jnp.bfloat16),
-                pltpu.VMEM((PARTS, SIDE, SUB, w), jnp.bfloat16),
-                pltpu.VMEM((PARTS, 2, SIDE, SUB, w), jnp.bfloat16),
-                pltpu.VMEM((PARTS, SIDE, SUB, w), jnp.bfloat16),
-                pltpu.VMEM((PARTS, 3, SUB, w), jnp.bfloat16),
-            ]
-    hidden = [pltpu.VMEM((PARTS, N_TP, 2, SUB, ff // 4), jnp.bfloat16) for _ in range(2)]
-    slots = [pltpu.VMEM((N_SP, CAP, features), jnp.bfloat16) for _ in range(4)]
-    return slots + hidden + per_part
-
-
-REDUCE = (("y", "x"), ("x", "y"))
+        target = scratch[3 + 5 * h]
+        here = place.on(SPREAD[h])
+        for n, matrix in enumerate((gate, up)):
+            into = pl.ds(n * quarter, quarter)
+            target[here, :, into] = matrix[:, pl.ds(pl.multiple_of(here * quarter, quarter), quarter)]
+            for off in (2, 1, -1):
+                columns = pl.ds(pl.multiple_of(place.on(SPREAD[h], off) * quarter, quarter), quarter)
+                copy = copies(
+                    matrix.at[:, columns], target.at[here, :, into], place.along(SPREAD[h], off)
+                )
+                copy.start()
+                sent.append(copy)
+    return sent
 
 
 def peers_along_z(place):
@@ -429,25 +460,29 @@
 
 
 def back(
-    place, copies,
-    mid_ref, gain_ref, pick_ref, high_ref, low_ref, gate_ref, up_ref, down_ref, out_ref, scratch,
+    place, copies, mid_ref, pick_ref, high_ref, low_ref, down_ref, out_ref, scratch,
 ):
-    outgoing, arrived, results, returned = scratch[:4]
-    hidden = scratch[4:6]
-    buffers = [[scratch[6 + (2 * h + q) * 5 : 11 + (2 * h + q) * 5] for q in range(2)] for h in range(2)]
+    outgoing, results, returned = scratch[:3]
+    weights, rows_in, products_of, others_of, hidden = zip(scratch[3:8], scratch[8:13])
     features = mid_ref.shape[1]
-    ff = gate_ref.shape[1]
-    half = ff // 2
+    quarter = hidden[0].shape[-1]
     z_peers = peers_along_z(place)
+
+    def landing(at):
+        part, i = at // POS, at % POS
+        h, i = i // (POS // 2), i % (POS // 2)
+        blocks = POS // 4
+        return rows_in[h].at[part, place.on(SPREAD[h]), i // blocks, pl.ds(i % blocks * CAP, CAP)]
+
     for part in range(PARTS):
         rows = pl.ds(part * POS * CAP, POS * CAP)
         outgoing[pl.ds(part * POS, POS)] = (
             dot(pick_ref[rows, :], mid_ref[...], NN).astype(jnp.bfloat16).reshape(POS, CAP, features)
         )
-    arrived[HOME] = outgoing[HOME]
+    landing(HOME)[...] = outgoing[HOME]
     dispatch = {}
     for at, there, device in z_peers:
-        dispatch[at] = copies(outgoing.at[at], arrived.at[there], device)
+        dispatch[at] = copies(outgoing.at[at], landing(there), device)
         dispatch[at].start()
     lands = {there: dispatch[at] for at, there, _ in z_peers}
     back = {}
@@ -456,106 +491,84 @@
         TorusGather(place, copies, [hidden[h].at[part] for h in range(2)]) for part in range(PARTS)
     ]
 
-    def add(*refs):
-        total = refs[0].astype(jnp.float32)
-        for ref in refs[1:]:
-            total += ref.astype(jnp.float32)
-        return total
-
-    def relay_out(part, h):
-        axis = REDUCE[h][0]
-        far = pl.ds(place.on(axis, 2) * SIDE, SIDE)
-        sent = []
-        for q, off in ((0, 1), (1, -1)):
-            product, passed = buffers[h][q][:2]
-            copy = copies(product.at[part, far], passed.at[part], place.along(axis, off))
-            copy.start()
-            sent.append(copy)
-        state[part][h, "relay"] = sent
-
-    def join(part, h):
-        axis = REDUCE[h][0]
-        sent = []
-        for side, off in ((0, 1), (1, -1)):
-            state[part][h, "relay"][side].wait_recv()
-            near = pl.ds(place.on(axis, off) * SIDE, SIDE)
-            for q in (1 - side, side):
-                product, passed, both = buffers[h][q][:3]
-                if q == side:
-                    product[part, near] = add(product[part, near], passed[part]).astype(jnp.bfloat16)
-                copy = copies(product.at[part, near], both.at[part, side], place.along(axis, off))
-                copy.start()
-                sent.append(copy)
-        state[part][h, "both"] = sent
-
-    def halfway(part, h):
-        first, second = REDUCE[h]
-        for copy in state[part][h, "both"]:
-            copy.wait_recv()
-        here = pl.ds(place.on(first) * SIDE, SIDE)
-        sent = []
-        for q in range(2):
-            product, _, both, reduced, others = buffers[h][q]
-            total = add(product[part, here], both[part, 0], both[part, 1])
-            reduced[part] = total.astype(jnp.bfloat16)
-            for side, off in enumerate((2, 1, -1)):
-                copy = copies(
-                    reduced.at[part, place.on(second, off)],
-                    others.at[part, side],
-                    place.along(second, off),
-                )
-                copy.start()
-                sent.append(copy)
-        state[part][h, "others"] = sent
-
-    def finish(part, h):
-        second = REDUCE[h][1]
-        for copy in state[part][h, "others"]:
-            copy.wait_recv()
-        return [
-            add(reduced[part, place.on(second)], *[others[part, side] for side in range(3)])
-            for _, _, _, reduced, others in buffers[h]
-        ]
-
-    def products(part):
+    def gather_rows(part):
         for at in range(part * POS, (part + 1) * POS):
             if at in lands:
                 lands[at].wait_recv()
-        rows = arrived[pl.ds(part * POS, POS)].reshape(POS * CAP, features).astype(jnp.float32)
-        squares = jnp.sum(rows * rows, axis=1, keepdims=True)
-        extra = jnp.broadcast_to(squares, (POS * CAP, EXTRA)).astype(jnp.bfloat16)
-        scaled = (rows * gain_ref[...]).astype(jnp.bfloat16)
         for h in range(2):
-            for q, matrix in enumerate((gate_ref, up_ref)):
-                value = dot(scaled, matrix[:, pl.ds(h * half, half)], NN).astype(jnp.bfloat16)
-                value = value.reshape(N_TP, SUB, half)
-                product = buffers[h][q][0]
-                for t, at in enumerate(torus_order(h)):
-                    product[part, at, :, pl.ds(0, half)] = value[t]
-                    if h == 0 and q == 0:
-                        product[part, at, :, pl.ds(half, EXTRA)] = extra[t * SUB : (t + 1) * SUB]
-            relay_out(part, h)
-
-    def activate(part):
-        (gate_a, up_a), (gate_b, up_b) = [finish(part, h) for h in range(2)]
-        inv = lax.rsqrt(gate_a[:, half : half + 1] * (1.0 / D) + EPS_NORM)
+            mine = rows_in[h].at[part, place.on(SPREAD[h])]
+            sent = [copies(mine, mine, place.along(SPREAD[h], off)) for off in (1, -1)]
+            for copy in sent:
+                copy.start()
+            state[part][h, "rows"] = sent
+
+    def relay_rows(part, h):
+        sent = []
+        for side, off in ((0, 1), (1, -1)):
+            state[part][h, "rows"][side].wait_recv()
+            piece = rows_in[h].at[part, place.on(SPREAD[h], -off), side]
+            sent.append(copies(piece, piece, place.along(SPREAD[h], off)))
+            sent[-1].start()
+        state[part][h, "relayed"] = sent
+
+    def multiply(part, h):
+        for copy in state[part][h, "relayed"]:
+            copy.wait_recv()
+        total, squares = 0.0, 0.0
+        for p in range(SIDE):
+            rows = rows_in[h][part, p].reshape(POS // 2 * CAP, features)
+            total += dot(rows, weights[h][p], NN)
+            squares += jnp.sum(jnp.square(rows.astype(jnp.float32)), axis=1, keepdims=True)
+        extra = jnp.broadcast_to(squares, (POS // 2 * CAP, EXTRA))
+        value = jnp.concatenate([total, extra], axis=1).astype(jnp.bfloat16)
+        products_of[h][part] = value.reshape(SIDE, SUB, 2 * quarter + EXTRA)
+        sent = []
+        for n, off in enumerate((2, 1, -1)):
+            sent.append(
+                copies(
+                    products_of[h].at[part, place.on(SUM[h], off)],
+                    others_of[h].at[part, n],
+                    place.along(SUM[h], off),
+                )
+            )
+            sent[-1].start()
+        state[part][h, "products"] = sent
+
+    def activate(part, h):
+        for copy in state[part][h, "products"]:
+            copy.wait_recv()
+        total = products_of[h][part, place.on(SUM[h])].astype(jnp.float32)
+        for n in range(3):
+            total += others_of[h][part, n].astype(jnp.float32)
+        inv = lax.rsqrt(total[:, 2 * quarter : 2 * quarter + 1] * (1.0 / D) + EPS_NORM)
+        gate = total[:, :quarter] * inv
+        value = gate * sigmoid(gate) * (total[:, quarter : 2 * quarter] * inv)
         gather = gathers[part]
-        for h, (gate, up) in enumerate(((gate_a[:, :half], up_a), (gate_b, up_b))):
-            gate = gate * inv
-            value = (gate * sigmoid(gate) * (up * inv)).astype(jnp.bfloat16)
-            for q in range(2):
-                hidden[h][part, gather.own(h), q] = value[:, q * (half // 2) : (q + 1) * (half // 2)]
-            gather.stage(0, h)
+        hidden[h][part, gather.at(h)] = value.astype(jnp.bfloat16).reshape(2, SUB // 2, quarter)
+        gather.begin(h)
+
+    def second_axis(part, h):
+        for off in (1, -1, 2):
+            gathers[part].arrive(h, off)
+        state[part][h, "pair"] = gathers[part].pair(h, gathers[part].row(h))
+
+    def relay_hidden(part, h):
+        gather = gathers[part]
+        state[part][h, "passed"] = gather.relay(
+            h, state[part][h, "pair"],
+            lambda second: gather.row(h, second), lambda ref, side: ref.at[:, side],
+        )
 
     def outputs(part):
-        total = jnp.zeros((POS * CAP, features), jnp.float32)
         for h in range(2):
-            gathers[part].stage(3, h)
-            for q in range(2):
-                blocks = [hidden[h][part, at, q] for at in torus_order(h)]
-                at = h * half + q * (half // 2)
-                total += dot(jnp.concatenate(blocks, axis=0), down_ref[pl.ds(at, half // 2), :], NN)
-        results[pl.ds(part * POS, POS)] = total.astype(jnp.bfloat16).reshape(POS, CAP, features)
+            for copy in state[part][h, "passed"]:
+                copy.wait_recv()
+            total = 0.0
+            for p in range(SIDE):
+                rows = hidden[h][part, pl.ds(p * SIDE, SIDE)].reshape(POS // 2 * CAP, quarter)
+                total += dot(rows, down_ref[pl.ds(p * quarter, quarter), :], NN)
+            first = part * POS + h * (POS // 2)
+            results[pl.ds(first, POS // 2)] = total.astype(jnp.bfloat16).reshape(POS // 2, CAP, features)
         for at, there, device in z_peers:
             if part * POS <= at < (part + 1) * POS:
                 back[at] = copies(results.at[at], returned.at[there], device)
@@ -570,12 +583,12 @@
         return run
 
     stages = [
-        products,
-        both(join),
-        both(halfway),
-        activate,
-        both(lambda part, h: gathers[part].stage(1, h)),
-        both(lambda part, h: gathers[part].stage(2, h)),
+        gather_rows,
+        both(relay_rows),
+        both(multiply),
+        both(activate),
+        both(second_axis),
+        both(relay_hidden),
         outputs,
     ]
     begins = (0.0, 7.0, 11.0, 13.0)
@@ -602,8 +615,8 @@
     ids_ref, route_weight_ref, mixer_hbm, gate_hbm, up_hbm, down_hbm, out_ref, *scratch
 ):
     mixer, gate, up, down, loaded, send, recv = scratch[:7]
-    reads, states, pick, high, low, midway, maps = scratch[7:14]
-    halves = scratch[14:16]
+    reads, states, pick, high, low, midway, cores, maps, incoming = scratch[7:16]
+    halves = scratch[16:18]
     place = Place()
     copies = Copies(send, recv)
     barrier = pltpu.get_barrier_semaphore()
@@ -628,19 +641,25 @@
         )
     pl.semaphore_wait(barrier, len(others))
 
-    def meanwhile():
-        route(place, ids_ref, route_weight_ref, pick, high, low)
+    spread = []
+
+    def prepare_weights():
         for load in loads:
             load.wait()
-
+        spread.extend(spread_weights(place, copies, norm_gain_ref, gate, up, scratch[18:]))
+
+    meanwhile = [
+        lambda: route(place, ids_ref, route_weight_ref, pick, high, low),
+        prepare_weights,
+    ]
     front(
         place, copies, meanwhile,
-        reads, states, gate_logits_ref, group_gain_ref, mixer, residual_ref, midway, maps, halves,
+        reads, states, gate_logits_ref, group_gain_ref, mixer, residual_ref, midway,
+        cores, maps, incoming, halves,
     )
-    back(
-        place, copies,
-        midway, norm_gain_ref, pick, high, low, gate, up, down, out_ref, scratch[16:],
-    )
+    for copy in spread:
+        copy.wait_recv()
+    back(place, copies, midway, pick, high, low, down, out_ref, scratch[18:])
     copies.drain()
 
 
@@ -665,7 +684,7 @@
     features = norm_gain.shape[0]
     ff = expert_gate.shape[2]
     slots = N_SP * CAP
-    count = 64 + 2 * (N_SP - 1) + PARTS * 40
+    count = 2 + (NZ - 1) + 12 + 38 + 2 * (N_SP - 1) + PARTS * 28
     bf16 = jnp.bfloat16
     vmem = pl.BlockSpec(memory_space=pltpu.VMEM)
     hbm = pl.BlockSpec(memory_space=pl.ANY)
@@ -686,7 +705,9 @@
             pltpu.VMEM((slots, tokens), bf16),
             pltpu.VMEM((slots, tokens), bf16),
             pltpu.VMEM((tokens, features), bf16),
-            pltpu.VMEM((N_SP, channels, 2 * HEAD), bf16),
+            pltpu.VMEM((2, channels, 2 * HEAD), bf16),
+            pltpu.VMEM((NZ, channels // 2, 2 * HEAD), bf16),
+            pltpu.VMEM((2, HEAD, channels // 2), jnp.float32),
             pltpu.VMEM((N_TP, 2, tokens // 4, channels), bf16),
             pltpu.VMEM((N_TP, 2, tokens // 4, channels), bf16),
         ]

time: 158 us -> 135 us (0.85)
  Pallas kernels: 157 us -> 133 us
    pallas_call x1, Pallas kernels: 157 us -> 133 us  [local(): pl.pallas_call(kernel, in_specs=[vmem] * 11 + [hbm] * 4, out_specs=vmem,...]
where the time goes in v3:
time: 135 us
  Pallas kernels  133 us (99%)
  local copies, waits for them, and re-layouts  1.57 us (1%)
    pallas_call x1, Pallas kernels, local(): pl.pallas_call(kernel, in_specs=[vmem] * 11 + [hbm] * 4, out_specs=vmem,...  133 us

profile of v3, /device:TPU:1, one launch (start us, length us, event | category | flops | bytes accessed | tf_op | source)
XLA Modules:
  0.0 134.6 jit_solution(13840445716765511469)
XLA Ops:
  0.0 133.1 %layer.1 = bf16[256,256]{1,0:T(8,128)(2,1)} custom-call(bf16[256,256]{1,0:T(8,128)(2,1)} %r_ref.1, bf16[256,256]{1,0:T(8,128)(2,1)} %k_ref.1, bf16[256,256]{1,0:T(8,128)(2,1)} %v_ref.1, bf16[256,256]{1,0:T(8,128)(2,1)} %d_ref.1, bf16[256,256]{1,0:T(8,128)(2,1)} %a_ref.1, bf16[256,256]{1,0:T(8,128)(2,1)} %gate_logits_ref.1, f32[1,256]{1,0:T(1,128)} %bitcast.12, ...), custom_call_target="tpu_custom_call" | custom-call | tf_op jit(solution)/shard_map/layer/pallas_call | solution.py:692
  133.1 1.6 %copy.17 = bf16[256,256]{1,0:T(8,128)(2,1)} copy(bf16[256,256]{1,0:T(8,128)(2,1)} %layer.1) | data formatting | bytes 262144

commit v4 on v3

--- a/solution.py
+++ b/solution.py
@@ -54,11 +54,26 @@
     return dot(a[0], b, dims) + dot(a[1], b, dims)
 
 
+def side(*parts):
+    return jnp.concatenate(parts, axis=1)
+
+
+def stack(*parts):
+    return jnp.concatenate(parts, axis=0)
+
+
+def packed(a, b):
+    width = b[0].shape[1]
+    both = side(*b)
+    total = dot(a, stack(both, both), NN)
+    return total[:, :width] + total[:, width:]
+
+
 def sigmoid(x):
     return 1.0 / (1.0 + jnp.exp(-x))
 
 
-def mix_kernel(r_ref, k_ref, v_ref, d_ref, a_ref, out_ref, state_ref):
+def mix(r_ref, k_ref, v_ref, d_ref, a_ref, out_ref, state_ref):
     tokens = r_ref.shape[0]
     chunks = tokens // CHUNK
     row = lax.broadcasted_iota(jnp.int32, (CHUNK, CHUNK), 0)
@@ -70,16 +85,17 @@
     low = lax.broadcasted_iota(jnp.int32, (CHUNK, 2 * HEAD), 1) < HEAD
 
     work = []
-    for chunk in range(chunks):
+    pairs = r_ref.shape[1] // (2 * HEAD)
+    for chunk, pair in [(c, p) for c in range(chunks) for p in range(pairs)]:
         rows = pl.ds(chunk * CHUNK, CHUNK)
-        recept = r_ref[rows, :].astype(jnp.float32)
-        keyvec = k_ref[rows, :].astype(jnp.float32)
-        logdec = -EXP_HALF * sigmoid(d_ref[rows, :].astype(jnp.float32))
+        wide = pl.ds(pair * 2 * HEAD, 2 * HEAD)
+        recept = r_ref[rows, wide].astype(jnp.float32)
+        keyvec = k_ref[rows, wide].astype(jnp.float32)
+        logdec = -EXP_HALF * sigmoid(d_ref[rows, wide].astype(jnp.float32))
         first, second = split(logdec)
         third = (logdec - first.astype(jnp.float32) - second.astype(jnp.float32)).astype(jnp.bfloat16)
-        cum_in = dot(ones_lower, first, NN) + (
-            dot(ones_lower, second, NN) + dot(ones_lower, third, NN)
-        )
+        cum_two = dot(ones_lower, side(first, second), NN)
+        cum_in = cum_two[:, : 2 * HEAD] + (cum_two[:, 2 * HEAD :] + dot(ones_lower, third, NN))
         cum_end = cum_in[CHUNK - 1 :, :]
         squares = keyvec * keyvec
         norms = jnp.where(
@@ -88,7 +104,7 @@
             jnp.sum(squares[:, HEAD:], axis=1, keepdims=True),
         )
         unit_key = keyvec * lax.rsqrt(1.0 + norms)
-        correction = unit_key * sigmoid(a_ref[rows, :].astype(jnp.float32))
+        correction = unit_key * sigmoid(a_ref[rows, wide].astype(jnp.float32))
         growth = jnp.exp(-cum_in)
         tail = jnp.exp(cum_end - cum_in)
         r_scaled = recept * jnp.exp(cum_in)
@@ -97,15 +113,15 @@
         sources = split(jnp.concatenate([keyvec * growth, correction * growth], axis=0))
         tails = split(jnp.concatenate([keyvec * tail, -(correction * tail)], axis=0))
         keep = jnp.broadcast_to(jnp.exp(cum_end), (2 * HEAD, 2 * HEAD)).T
-        values = v_ref[rows, :]
+        values = v_ref[rows, wide]
         for head in range(2):
             lanes = slice(head * HEAD, (head + 1) * HEAD)
-            query = tuple(q[:, lanes] for q in queries)
-            source = tuple(s[:, lanes] for s in sources)
-            scores = dot3(query, source, NT)
+            query = side(*[q[:, lanes] for q in queries])
+            near, rest = [s[:, lanes] for s in sources]
+            scores = dot(side(query, query), side(near, near, rest, rest), NT)
             work.append(
                 dict(
-                    head=head,
+                    head=pair * 2 + head,
                     chunk=chunk,
                     query=query,
                     tail=tuple(t[:, lanes] for t in tails),
@@ -128,7 +144,7 @@
             )
     for item in work:
         item["inverse"] = eye - jnp.where(row // 2 == col // 2, item["pull"], 0.0)
-        item["from_values"] = dot2(item["key_both"], item["value"])
+        item["from_values"] = dot(side(*item["key_both"]), stack(item["value"], item["value"]), NN)
     size = 2
     while size < CHUNK:
         joined = (row // (2 * size) == col // (2 * size)) & (row // size != col // size)
@@ -136,22 +152,22 @@
         for item in work:
             inverse = split(item["inverse"])
             between = split(jnp.where(joined, item["pull"], 0.0))
-            halves.append((inverse, dot3(between, inverse)))
+            halves.append((inverse, packed(side(*between), inverse)))
         for item, (inverse, half) in zip(work, halves):
-            item["inverse"] = item["inverse"] - dot3(inverse, split(half))
+            item["inverse"] = item["inverse"] - packed(side(*inverse), split(half))
         size *= 2
     key_row = lax.broadcasted_iota(jnp.int32, (HEAD, 2 * HEAD), 0)
     lane = lax.broadcasted_iota(jnp.int32, (HEAD, 2 * HEAD), 1)
     start = jnp.where(lane == key_row + HEAD, 1.0, 0.0)
-    states = [start, start]
+    states = [start] * (2 * pairs)
     for item in work:
         head = item["head"]
         state = states[head]
-        from_start = dot3(item["query"], split(state)) + item["from_values"]
-        pulled = dot3(split(item["inverse"]), split(from_start[:CHUNK]))
+        from_start = packed(item["query"], split(state)) + item["from_values"]
+        pulled = packed(side(*split(item["inverse"])), split(from_start[:CHUNK]))
         pulled_parts = split(pulled)
         out_ref[pl.ds(item["chunk"] * CHUNK, CHUNK), pl.ds(head * 2 * HEAD, 2 * HEAD)] = (
-            from_start[CHUNK:] - dot3(item["corr_read"], pulled_parts)
+            from_start[CHUNK:] - packed(side(*item["corr_read"]), pulled_parts)
         )
         key_tail = tuple(t[:CHUNK] for t in item["tail"])
         corr_tail = tuple(t[CHUNK:] for t in item["tail"])
@@ -160,7 +176,7 @@
             + dot2(key_tail, item["value"], TN)
             + dot3(corr_tail, pulled_parts, TN)
         )
-    for head in range(2):
+    for head in range(2 * pairs):
         state_ref[pl.ds(head * HEAD, HEAD), :] = states[head].astype(jnp.bfloat16)
 
 
@@ -314,33 +330,54 @@
                 came[direction, d + far] = copies(ref, ref, place.at_z(direction * far))
                 came[direction, d + far].start()
 
+    def step_of(d, head):
+        both = maps[(place.z - d + NZ) % NZ, pl.ds(head * HEAD, HEAD), :]
+        return jnp.where(place.z >= d, both, unit)
+
+    lane = lax.broadcasted_iota(jnp.int32, (HEAD, 2 * HEAD), 1)
+    row = lax.broadcasted_iota(jnp.int32, (HEAD, 2 * HEAD), 0)
+    identity = jnp.where(lane == row + HEAD, 1.0, 0.0)
+    unit = identity.astype(jnp.bfloat16)
+    window = [identity] * mine
+    far = [jnp.zeros((HEAD, HEAD), jnp.float32)] * mine
+
+    def take(direction, d):
+        for head in range(mine):
+            if direction > 0:
+                both = step_of(d, head)
+                hi, lo = split(window[head][:, HEAD:])
+                added = dot(hi, both, NN) + dot(lo, both, NN)
+                window[head] = side(window[head][:, :HEAD] + added[:, :HEAD], added[:, HEAD:])
+            else:
+                both = step_of(NZ - d, head)
+                hi, lo = split(far[head])
+                step_map = both[:, HEAD:]
+                far[head] = (
+                    both[:, :HEAD].astype(jnp.float32) + dot(step_map, hi, NN) + dot(step_map, lo, NN)
+                )
+
     for d in range(0, NZ // 2, 2):
         for direction in (1, -1):
             if d:
                 came[direction, d].wait_recv()
             pass_on(direction, d)
+        if d:
+            for direction in (1, -1):
+                came[direction, d - 1].wait_recv()
+                take(direction, d - 1)
+                take(direction, d)
         if d // 2 < len(meanwhile):
             meanwhile[d // 2]()
     for direction in (1, -1):
-        for d in range(1, last[direction] + 1):
-            if d % 2 or d == NZ // 2:
+        for d in (NZ // 2 - 1, NZ // 2):
+            if d <= last[direction]:
                 came[direction, d].wait_recv()
-
-    def fold(step, carried):
-        following = []
-        for head in range(mine):
-            both = maps[step, pl.ds(head * HEAD, HEAD), :]
-            hi, lo = split(carried[head])
-            step_map = both[:, HEAD:]
-            following.append(
-                both[:, :HEAD].astype(jnp.float32) + dot(step_map, hi, NN) + dot(step_map, lo, NN)
-            )
-        return tuple(following)
-
-    zero = jnp.zeros((HEAD, HEAD), jnp.float32)
-    incoming_ref[place.core] = jnp.concatenate(
-        lax.fori_loop(0, place.z, fold, (zero,) * mine), axis=1
-    )
+                take(direction, d)
+    incoming = [
+        window[head][:, :HEAD] + dot3(split(window[head][:, HEAD:]), split(far[head]))
+        for head in range(mine)
+    ]
+    incoming_ref[place.core] = side(*incoming)
     swap = copies(incoming_ref.at[place.core], incoming_ref.at[place.core], partner)
     swap.start()
     second = (jnp.zeros((HEAD, HEAD), jnp.int32) + place.core) == 1
@@ -474,16 +511,17 @@
         blocks = POS // 4
         return rows_in[h].at[part, place.on(SPREAD[h]), i // blocks, pl.ds(i % blocks * CAP, CAP)]
 
+    dispatch = {}
     for part in range(PARTS):
         rows = pl.ds(part * POS * CAP, POS * CAP)
         outgoing[pl.ds(part * POS, POS)] = (
             dot(pick_ref[rows, :], mid_ref[...], NN).astype(jnp.bfloat16).reshape(POS, CAP, features)
         )
+        for at, there, device in z_peers:
+            if part * POS <= at < (part + 1) * POS:
+                dispatch[at] = copies(outgoing.at[at], landing(there), device)
+                dispatch[at].start()
     landing(HOME)[...] = outgoing[HOME]
-    dispatch = {}
-    for at, there, device in z_peers:
-        dispatch[at] = copies(outgoing.at[at], landing(there), device)
-        dispatch[at].start()
     lands = {there: dispatch[at] for at, there, _ in z_peers}
     back = {}
     state = [dict() for _ in range(PARTS)]
@@ -607,7 +645,7 @@
         rows = returned[pl.ds(part * POS, POS)].reshape(POS * CAP, features)
         columns = pl.ds(part * POS * CAP, POS * CAP)
         total += dot(high_ref[columns, :], rows, TN) + dot(low_ref[columns, :], rows, TN)
-    out_ref[...] = total.astype(jnp.bfloat16)
+    out_ref[...] = total
 
 
 def kernel(
@@ -632,13 +670,7 @@
     ]
     for load in loads:
         load.start()
-    for pair in range(r_ref.shape[1] // (2 * HEAD)):
-        lanes = pl.ds(pair * 2 * HEAD, 2 * HEAD)
-        mix_kernel(
-            *[ref.at[:, lanes] for ref in (r_ref, k_ref, v_ref, d_ref, a_ref)],
-            reads.at[:, pl.ds(pair * 4 * HEAD, 4 * HEAD)],
-            states.at[lanes, :],
-        )
+    mix(r_ref, k_ref, v_ref, d_ref, a_ref, reads, states)
     pl.semaphore_wait(barrier, len(others))
 
     spread = []
@@ -693,7 +725,7 @@
         kernel,
         in_specs=[vmem] * 11 + [hbm] * 4,
         out_specs=vmem,
-        out_shape=jax.ShapeDtypeStruct((tokens, features), bf16),
+        out_shape=jax.ShapeDtypeStruct((tokens, features), jnp.float32),
         scratch_shapes=[pltpu.VMEM(w.shape, bf16) for w in weights]
         + [
             pltpu.SemaphoreType.DMA((len(weights),)),
@@ -720,7 +752,7 @@
         receptance, key_vectors, value_vectors, decay_logits, rate_logits, gate_logits,
         group_gain.reshape(1, channels), residual, norm_gain.reshape(1, features),
         expert_ids.T, route_weight.T, *weights,
-    )
+    ).astype(bf16)
 
 
 def solution(mesh):

time: 135 us -> 130 us (0.963)
  Pallas kernels: 133 us -> 129 us
  other arithmetic: 0 us -> 1.62 us
  local copies, waits for them, and re-layouts: 1.57 us -> 0 us
    pallas_call x1, Pallas kernels: 133 us -> 129 us  [local(): pl.pallas_call(kernel, in_specs=[vmem] * 11 + [hbm] * 4, out_specs=vmem,...]
    convert_element_type x0 -> x1, other arithmetic: none -> 1.62 us  [local(): return pl.pallas_call(kernel, in_specs=[vmem] * 11 + [hbm] * 4, out_specs...]
    unnamed x1 -> x0, local copies, waits for them, and re-layouts: 1.57 us -> none
where the time goes in v4:
time: 130 us
  Pallas kernels  129 us (99%)
  other arithmetic  1.62 us (1%)
    pallas_call x1, Pallas kernels, local(): pl.pallas_call(kernel, in_specs=[vmem] * 11 + [hbm] * 4, out_specs=vmem,...  129 us

profile of v4, /device:TPU:1, one launch (start us, length us, event | category | flops | bytes accessed | tf_op | source)
XLA Modules:
  0.0 130.3 jit_solution(589502956735167188)
XLA Ops:
  0.0 128.7 %layer.1 = f32[256,256]{1,0:T(8,128)} custom-call(bf16[256,256]{1,0:T(8,128)(2,1)} %r_ref.1, bf16[256,256]{1,0:T(8,128)(2,1)} %k_ref.1, bf16[256,256]{1,0:T(8,128)(2,1)} %v_ref.1, bf16[256,256]{1,0:T(8,128)(2,1)} %d_ref.1, bf16[256,256]{1,0:T(8,128)(2,1)} %a_ref.1, bf16[256,256]{1,0:T(8,128)(2,1)} %gate_logits_ref.1, f32[1,256]{1,0:T(1,128)} %bitcast.12, ...), custom_call_target="tpu_custom_call" | custom-call | tf_op jit(solution)/shard_map/layer/pallas_call | solution.py:724
  128.7 1.6 %convert_element_type.3 = bf16[256,256]{1,0:T(8,128)(2,1)} convert(f32[256,256]{1,0:T(8,128)} %layer.1) | non-fusion elementwise | flops 65536 | bytes 393216 | tf_op jit(solution)/shard_map/convert_element_type | solution.py:755

commit v5 on v4

--- a/solution.py
+++ b/solution.py
@@ -530,10 +530,11 @@
     ]
 
     def gather_rows(part):
-        for at in range(part * POS, (part + 1) * POS):
-            if at in lands:
-                lands[at].wait_recv()
         for h in range(2):
+            first = part * POS + h * (POS // 2)
+            for at in range(first, first + POS // 2):
+                if at in lands:
+                    lands[at].wait_recv()
             mine = rows_in[h].at[part, place.on(SPREAD[h])]
             sent = [copies(mine, mine, place.along(SPREAD[h], off)) for off in (1, -1)]
             for copy in sent:
@@ -607,10 +608,10 @@
                 total += dot(rows, down_ref[pl.ds(p * quarter, quarter), :], NN)
             first = part * POS + h * (POS // 2)
             results[pl.ds(first, POS // 2)] = total.astype(jnp.bfloat16).reshape(POS // 2, CAP, features)
-        for at, there, device in z_peers:
-            if part * POS <= at < (part + 1) * POS:
-                back[at] = copies(results.at[at], returned.at[there], device)
-                back[at].start()
+            for at, there, device in z_peers:
+                if first <= at < first + POS // 2:
+                    back[at] = copies(results.at[at], returned.at[there], device)
+                    back[at].start()
         if part == HOME // POS:
             returned[HOME] = results[HOME]
 

time: 130 us -> 129 us (level)
  no operation moved by 1% of the time
where the time goes in v5:
time: 129 us
  Pallas kernels  128 us (99%)
  other arithmetic  1.62 us (1%)
    pallas_call x1, Pallas kernels, local(): pl.pallas_call(kernel, in_specs=[vmem] * 11 + [hbm] * 4, out_specs=vmem,...  128 us

profile of v5, /device:TPU:1, one launch (start us, length us, event | category | flops | bytes accessed | tf_op | source)
XLA Modules:
  0.0 129.2 jit_solution(6886439057723359300)
XLA Ops:
  0.0 127.6 %layer.1 = f32[256,256]{1,0:T(8,128)} custom-call(bf16[256,256]{1,0:T(8,128)(2,1)} %r_ref.1, bf16[256,256]{1,0:T(8,128)(2,1)} %k_ref.1, bf16[256,256]{1,0:T(8,128)(2,1)} %v_ref.1, bf16[256,256]{1,0:T(8,128)(2,1)} %d_ref.1, bf16[256,256]{1,0:T(8,128)(2,1)} %a_ref.1, bf16[256,256]{1,0:T(8,128)(2,1)} %gate_logits_ref.1, f32[1,256]{1,0:T(1,128)} %bitcast.12, ...), custom_call_target="tpu_custom_call" | custom-call | tf_op jit(solution)/shard_map/layer/pallas_call | solution.py:725
  127.6 1.6 %convert_element_type.3 = bf16[256,256]{1,0:T(8,128)(2,1)} convert(f32[256,256]{1,0:T(8,128)} %layer.1) | non-fusion elementwise | flops 65536 | bytes 393216 | tf_op jit(solution)/shard_map/convert_element_type | solution.py:756
